TPU v7x, 32 devices: a whole 2x2x4 slice. The times are simulated.
32 devices in a mesh: fs: 8 (over z, x), tp: 4 (over y, core).
Axes of the slice: x: 2, y: 2, z: 4, core: 2. Of those that a mesh axis runs over, the one named last changes fastest.
Arguments:
- tokens: bfloat16 [2048, 3072], P('tp', 'fs'), may hold values from -6 to 6
- mix_gain: float32 [2048], replicated, may hold values from 0.1 to 1.9
- mlp_gain: float32 [2048], replicated, may hold values from 0.1 to 1.9
- query_weight: float32 [2048, 1024], P('fs', 'tp'), may hold values from -0.125 to 0.125
- key_weight: float32 [2048, 1024], P('fs', 'tp'), may hold values from -0.125 to 0.125
- value_weight: float32 [2048, 1024], P('fs', 'tp'), may hold values from -0.125 to 0.125
- gate_weight: float32 [2048, 1024], P('fs', 'tp'), may hold values from -0.125 to 0.125
- out_weight: float32 [1024, 2048], P('tp', 'fs'), may hold values from -0.1875 to 0.1875
- up_weight: float32 [2048, 8192], P('fs', 'tp'), may hold values from -0.125 to 0.125
- down_weight: float32 [8192, 2048], P('tp', 'fs'), may hold values from -0.0625 to 0.0625
- query_scale: float32 [1024], P(('tp', 'fs')), may hold values from 0.1 to 1.9
- key_scale: float32 [1024], P(('tp', 'fs')), may hold values from 0.1 to 1.9
- value_scale: float32 [1024], P(('tp', 'fs')), may hold values from 0.1 to 1.9
- gate_scale: float32 [1024], P(('tp', 'fs')), may hold values from 0.1 to 1.9
- out_scale: float32 [2048], P(('tp', 'fs')), may hold values from 0.1 to 1.9
- up_scale: float32 [8192], P(('tp', 'fs')), may hold values from 0.1 to 1.9
- down_scale: float32 [2048], P(('tp', 'fs')), may hold values from 0.1 to 1.9
- forget: float32 [16], P('tp'), as said below
Outputs:
- layer_out: bfloat16 [2048, 3072], P('tp', 'fs')
Inputs may be any that keep to these rules, and one draw needn't show every extreme that they name: `forget`: positive rates; each head either forgets within a few tens of positions or keeps a tenth or more over a whole sequence of 384.
All inputs are finite; a program needn't handle non-finite values.
Results may differ from a plain program's by a relative error of at most 0.02.
Values may be sent and summed in bfloat16 or wider, within the bound.
A program may use at most 64 MiB of HBM per device.

v0:
```python
import functools

import jax
import jax.numpy as jnp
import numpy as np
from jax import lax
from jax.experimental import pallas as pl
from jax.experimental.pallas import tpu as pltpu
from jax.sharding import PartitionSpec as P

MESH = pl.DeviceIdType.MESH
BF = jnp.bfloat16
F32 = jnp.float32


def nn(a, b):
    return lax.dot_general(a, b, (((1,), (0,)), ((), ())), preferred_element_type=F32)


def nt(a, b):
    return lax.dot_general(a, b, (((1,), (1,)), ((), ())), preferred_element_type=F32)


def kernel(cfg, *refs):
    Z, X, Y, C, G, heads = cfg
    n_tp = Y * C
    n_w = 4
    tok, gains, scales, cos_t, sin_t, forget = refs[:6]
    own = refs[6 : 6 + n_w]
    out_ref = refs[6 + n_w]
    rest = refs[7 + n_w :]
    full = rest[:n_w]
    (scale_g, scale_row, tok_g, seqs, parts, core_in, y_out, y_in, z_out, z_in, normed, proj, mixed, hidden,
     local_sem, zs, zr, xs, xr, ts, tr, azs, azr, ays, ayr, acs, acr, rcs, rcr, rys, ryr, rzs, rzr) = rest[n_w:]
    me = lax.axis_index("fs")
    tp = lax.axis_index("tp")
    z = me // X
    x = lax.rem(me, X)
    y = tp // C
    core = lax.rem(tp, C)
    length, width = tok.shape
    ret = mixed.shape[1]
    head = ret // heads

    def at_z(o):
        return lax.rem(z + o, Z) * X + x

    def at_g(o):
        return (z // G * G + lax.rem(z + o, G)) * X + x

    def at_x(o):
        return z * X + lax.rem(x + o, X)

    def at_tp(o):
        return lax.rem(tp + o, n_tp)

    def at_y(o):
        return lax.rem(y + o, Y) * C + core

    def at_core(o):
        return y * C + lax.rem(core + o, C)

    barrier = pltpu.get_barrier_semaphore()
    for o in range(1, Z):
        pl.semaphore_signal(barrier, inc=1, device_id={"fs": at_z(o)}, device_id_type=MESH)
    for o in range(1, X):
        pl.semaphore_signal(barrier, inc=1, device_id={"fs": at_x(o)}, device_id_type=MESH)
    for o in range(1, n_tp):
        pl.semaphore_signal(barrier, inc=1, device_id={"tp": at_tp(o)}, device_id_type=MESH)
    pl.semaphore_wait(barrier, Z - 1 + X - 1 + n_tp - 1)

    pending = []

    def remote(src, dst, ss, rs, where):
        return pltpu.make_async_remote_copy(
            src_ref=src, dst_ref=dst, send_sem=ss, recv_sem=rs, device_id=where, device_id_type=MESH
        )

    def send(*parts_of):
        copy = remote(*parts_of)
        copy.start()
        pending.append(copy)

    def place(w, owner):
        if w == n_w:
            return scale_g.at[owner]
        rows = own[w].shape[-2]
        return full[w].at[pl.ds(pl.multiple_of(owner * rows, rows), rows)]

    def mine(w, o):
        if w == n_w:
            return scales
        return own[w].at[lax.rem(z + o, G)] if w >= 2 else own[w]

    def z_send(w):
        for o in range(1, Z):
            send(mine(w, o), place(w, me), zs.at[w, o - 1], zr.at[w, o - 1], {"fs": at_z(o)})

    def x_own(w):
        for o in range(1, X):
            send(mine(w, 0), place(w, me), xs.at[w, 0, o - 1], xr.at[w, 0, o - 1], {"fs": at_x(o)})

    def relay(w):
        for k in range(1, Z):
            piece = place(w, at_z(Z - k))
            remote(piece, piece, zs.at[w, k - 1], zr.at[w, k - 1], {"fs": at_z(k)}).wait_recv()
            for o in range(1, X):
                send(piece, piece, xs.at[w, k, o - 1], xr.at[w, k, o - 1], {"fs": at_x(o)})

    def finish(w):
        for k in range(Z):
            for o in range(1, X):
                owner = lax.rem(z + Z - k, Z) * X + lax.rem(x + X - o, X)
                piece = place(w, owner)
                remote(piece, piece, xs.at[w, k, o - 1], xr.at[w, k, o - 1], {"fs": at_x(o)}).wait_recv()

    def store_parts(k, t, value):
        parts[k, t % C, t // C] = value.astype(BF)

    def reduce_start(k):
        for o in range(1, C):
            send(parts.at[k, lax.rem(core + o, C)], core_in.at[k, o - 1], rcs.at[k, o - 1], rcr.at[k, o - 1],
                 {"tp": at_core(o)})

    def reduce_core(k):
        for o in range(1, C):
            slot = core_in.at[k, o - 1]
            remote(slot, slot, rcs.at[k, o - 1], rcr.at[k, o - 1], {"tp": at_core(o)}).wait_recv()
        for j in range(Y):
            value = parts[k, core, j].astype(F32)
            for o in range(1, C):
                value += core_in[k, o - 1, j].astype(F32)
            y_out[k, j] = value.astype(BF)
        for j in range(1, Y):
            send(y_out.at[k, lax.rem(y + j, Y)], y_in.at[k, j - 1], rys.at[k, j - 1], ryr.at[k, j - 1],
                 {"tp": at_y(j)})

    def reduce_y(k):
        value = y_out[k, y].astype(F32)
        for j in range(1, Y):
            slot = y_in.at[k, j - 1]
            remote(slot, slot, rys.at[k, j - 1], ryr.at[k, j - 1], {"tp": at_y(j)}).wait_recv()
            value += y_in[k, j - 1].astype(F32)
        return value

    def norm(block, row):
        square = jnp.zeros((length, 1), F32)
        for t in range(n_tp):
            v = block(t)[...].astype(F32)
            square += jnp.sum(v * v, axis=-1, keepdims=True)
        factor = lax.rsqrt(square / (width * n_tp) + 1e-6)
        for t in range(n_tp):
            cols = slice(t * width, (t + 1) * width)
            normed[:, cols] = (block(t)[...].astype(F32) * factor * gains[row : row + 1, cols]).astype(BF)

    for o in range(1, n_tp):
        send(tok, tok_g.at[tp], ts.at[o - 1], tr.at[o - 1], {"tp": at_tp(o)})
    for w in (n_w, 0, 1):
        z_send(w)
        x_own(w)
    locals_ = [pltpu.make_async_copy(mine(w, 0), place(w, me), local_sem.at[w]) for w in range(n_w + 1)]
    locals_.append(pltpu.make_async_copy(tok, tok_g.at[tp], local_sem.at[n_w + 1]))
    for copy in locals_:
        copy.start()
    for copy in locals_:
        copy.wait()
    for o in range(1, n_tp):
        slot = tok_g.at[at_tp(n_tp - o)]
        remote(slot, slot, ts.at[o - 1], tr.at[o - 1], {"tp": at_tp(o)}).wait_recv()
    norm(lambda t: tok_g.at[t], 0)

    relay(n_w)
    relay(0)
    relay(1)
    z_send(2)
    finish(n_w)
    finish(0)
    x_own(2)
    scale = jnp.sum(scale_g[...], axis=0)
    scale_row[...] = scale
    at = 4 * ret
    out_scale = scale[:, at : at + width]
    down_scale = scale[:, at + width : at + 2 * width]
    up_at = at + 2 * width

    for i in range(4):
        piece = nn(normed[...], full[0][:, i * ret : (i + 1) * ret])
        proj[i] = (piece * scale[:, i * ret : (i + 1) * ret]).astype(BF)

    r = lax.broadcasted_iota(jnp.int32, (ret, ret), 0)
    c = lax.broadcasted_iota(jnp.int32, (ret, ret), 1)
    odd = lax.rem(c, 2) == 1
    swap = jnp.where((r == c - 1) & odd, 1.0, jnp.where((r == c + 1) & ~odd, -1.0, 0.0)).astype(BF)
    same = jnp.where(r // head == c // head, 1.0 / head, 0.0).astype(F32)

    def turn(field):
        return field.astype(F32) * cos_t[...] + nn(field, swap) * sin_t[...]

    rot_q = turn(proj[0])
    rot_k = (turn(proj[1]) * head ** (-0.5)).astype(BF)
    vals = proj[2]
    rows = lax.broadcasted_iota(jnp.int32, (length, length), 0)
    cols = lax.broadcasted_iota(jnp.int32, (length, length), 1)
    dist = (rows - cols).astype(F32)
    lane = lax.broadcasted_iota(jnp.int32, (length, ret), 1) // head
    total = jnp.zeros((length, ret), F32)
    for h in range(heads):
        q_h = jnp.where(lane == h, rot_q, 0.0).astype(BF)
        decay = jnp.where(dist >= 0.0, jnp.exp(-forget[h] * jnp.maximum(dist, 0.0)), 0.0)
        inner = (nt(q_h, rot_k) * decay).astype(BF)
        total = jnp.where(lane == h, nn(inner, vals), total)
    mean = lax.dot_general(
        total * total, same, (((1,), (0,)), ((), ())), precision=lax.Precision.HIGHEST, preferred_element_type=F32
    )
    gate = proj[3].astype(F32)
    mixed[...] = (gate / (1.0 + jnp.exp(-gate)) * (total * lax.rsqrt(mean + 0.01))).astype(BF)

    finish(1)
    x_own(3)
    for t in range(n_tp):
        store_parts(G, t, nt(mixed[...], full[1][t * width : (t + 1) * width, :]))
    reduce_start(G)
    reduce_core(G)
    after = (tok[...].astype(F32) + reduce_y(G) * out_scale).astype(BF)
    seqs[0, tp] = after

    for k in range(1, G):
        send(seqs.at[0, tp], seqs.at[k, tp], azs.at[k - 1], azr.at[k - 1], {"fs": at_g(k)})

    def collect_z(k):
        slot = seqs.at[k, tp]
        if k:
            remote(slot, slot, azs.at[k - 1], azr.at[k - 1], {"fs": at_g(k)}).wait_recv()
        for j in range(1, Y):
            send(slot, slot, ays.at[k, j - 1], ayr.at[k, j - 1], {"tp": at_y(j)})
        for o in range(1, C):
            send(slot, slot, acs.at[k, 0, o - 1], acr.at[k, 0, o - 1], {"tp": at_core(o)})

    def collect_y(k):
        for j in range(1, Y):
            slot = seqs.at[k, at_y(Y - j)]
            remote(slot, slot, ays.at[k, j - 1], ayr.at[k, j - 1], {"tp": at_y(j)}).wait_recv()
            for o in range(1, C):
                send(slot, slot, acs.at[k, j, o - 1], acr.at[k, j, o - 1], {"tp": at_core(o)})

    def feed(k):
        for j in range(Y):
            for o in range(1, C):
                slot = seqs.at[k, lax.rem(y + Y - j, Y) * C + lax.rem(core + C - o, C)]
                remote(slot, slot, acs.at[k, j, o - 1], acr.at[k, j, o - 1], {"tp": at_core(o)}).wait_recv()
        norm(lambda t: seqs.at[k, t], 1)

    def expand(k):
        chunk = hidden.shape[2]
        step = 256 if chunk % 256 == 0 else chunk

        def tile(i, carry):
            here = pl.ds(pl.multiple_of(i * step, step), step)
            s = scale_row[:, pl.ds(pl.multiple_of(up_at + lax.rem(z, G) * chunk + i * step, 128), step)]
            u = jnp.maximum(nn(normed[...], full[2][:, here]) * s, 0.0)
            hidden[k, :, here] = (u * u).astype(BF)
            return carry

        lax.fori_loop(0, chunk // step, tile, 0)

    def shrink(k):
        for t in range(n_tp):
            store_parts(k, t, nt(hidden[k], full[3][t * width : (t + 1) * width, :]))
        reduce_start(k)

    def give_z(k):
        value = reduce_y(k)
        z_out[k] = value.astype(BF)
        if k:
            send(z_out.at[k], z_in.at[k - 1], rzs.at[k - 1], rzr.at[k - 1], {"fs": at_g(G - k)})

    collect_z(0)
    relay(2)
    for k in range(1, G):
        collect_z(k)
    z_send(3)
    collect_y(0)
    feed(0)
    finish(2)
    expand(0)
    for k in range(1, G):
        collect_y(k)
        feed(k)
        expand(k)
    relay(3)
    finish(3)
    order = list(range(1, G)) + [0]
    for k in order:
        shrink(k)
    for k in order:
        reduce_core(k)
    for k in order:
        give_z(k)
    mlp_total = z_out[0].astype(F32)
    for k in range(1, G):
        slot = z_in.at[k - 1]
        remote(slot, slot, rzs.at[k - 1], rzr.at[k - 1], {"fs": at_g(k)}).wait_recv()
        mlp_total += z_in[k - 1].astype(F32)
    out_ref[...] = (seqs[0, tp].astype(F32) + mlp_total * down_scale).astype(BF)
    for copy in pending:
        copy.wait_send()


def tables(length, head, heads):
    half = head // 2
    inverse = 1.0 / 10000.0 ** np.linspace(0.0, 1.0, half)
    angle = np.arange(length)[:, None] * inverse.astype(np.float32).astype(np.float64)[None, :]
    spread = lambda a: np.tile(np.repeat(a, 2, axis=1), (1, heads)).astype(np.float32)
    return spread(np.cos(angle)), spread(np.sin(angle))


def solution(mesh):
    n_fs, n_tp = mesh.shape["fs"], mesh.shape["tp"]
    heights = [getattr(d, "coords", (0, 0, i))[2] for i, d in enumerate(mesh.devices[:, 0])]
    X = heights.count(heights[0])
    if n_fs % X:
        X = 1
    Z = n_fs // X
    cores = [getattr(d, "core_on_chip", 0) for d in mesh.devices[0]]
    C = len(set(cores))
    if n_tp % C:
        C = 1
    Y = n_tp // C
    G = 2 if Z % 2 == 0 else Z

    def on_device(tokens, mix_gain, mlp_gain, wq, wk, wv, wg, wo, wu, wd, sq, sk, sv, sg, so, su, sd, forget):
        width, length = tokens.shape
        D = width * n_tp
        ret = wq.shape[1]
        heads = forget.shape[0]
        ff = wu.shape[1]
        chunk = ff // G
        me = lax.axis_index("fs")

        def spot(s):
            wide = jnp.tile(s, n_fs)
            return jnp.where(jnp.arange(wide.shape[0]) // s.shape[0] == me, wide, 0.0)

        scales = jnp.concatenate([spot(s) for s in (sq, sk, sv, sg, so, sd, su)])[None, :]
        gains = jnp.stack([mix_gain, mlp_gain])
        cos_t, sin_t = tables(length, ret // heads, heads)
        own = [jnp.concatenate([w.astype(BF) for w in (wq, wk, wv, wg)], axis=1), wo.astype(BF).T]
        own.append(wu.astype(BF).reshape(-1, G, chunk).transpose(1, 0, 2))
        own.append(wd.astype(BF).reshape(G, chunk, -1).transpose(0, 2, 1))
        n_w = len(own)
        vm = pl.BlockSpec(memory_space=pltpu.VMEM)
        dma = pltpu.SemaphoreType.DMA
        tile = (length, width)
        scratch = [pltpu.VMEM((n_fs * w.shape[-2], w.shape[-1]), BF) for w in own]
        scratch += [
            pltpu.VMEM((n_fs,) + scales.shape, F32),
            pltpu.VMEM(scales.shape, F32),
            pltpu.VMEM((n_tp,) + tile, BF),
            pltpu.VMEM((G, n_tp) + tile, BF),
            pltpu.VMEM((G + 1, C, Y) + tile, BF),
            pltpu.VMEM((G + 1, C - 1, Y) + tile, BF),
            pltpu.VMEM((G + 1, Y) + tile, BF),
            pltpu.VMEM((G + 1, Y - 1) + tile, BF),
            pltpu.VMEM((G,) + tile, BF),
            pltpu.VMEM((G - 1,) + tile, BF),
            pltpu.VMEM((length, D), BF),
            pltpu.VMEM((4, length, ret), BF),
            pltpu.VMEM((length, ret), BF),
            pltpu.VMEM((G, length, chunk), BF),
            dma((n_w + 2,)),
        ]
        for shape in [(n_w + 1, Z - 1), (n_w + 1, Z, X - 1), (n_tp - 1,), (G - 1,), (G, Y - 1), (G, Y, C - 1),
                      (G + 1, C - 1), (G + 1, Y - 1), (G - 1,)]:
            scratch += [dma(shape), dma(shape)]
        out = pl.pallas_call(
            functools.partial(kernel, (Z, X, Y, C, G, heads)),
            out_shape=jax.ShapeDtypeStruct((length, width), BF),
            in_specs=[vm] * 5 + [pl.BlockSpec(memory_space=pltpu.SMEM)] + [vm] * n_w,
            out_specs=vm,
            scratch_shapes=scratch,
            compiler_params=pltpu.CompilerParams(
                collective_id=0, has_side_effects=True, vmem_limit_bytes=60 * 2**20
            ),
            name="layer",
        )(tokens.T, gains, scales, jnp.asarray(cos_t), jnp.asarray(sin_t), forget, *own)
        return out.T

    cut = P(("tp", "fs"))
    rows, cols = P("fs", "tp"), P("tp", "fs")
    in_specs = (cols, P(), P(), rows, rows, rows, rows, cols, rows, cols) + (cut,) * 7 + (P("tp"),)
    return jax.shard_map(on_device, mesh=mesh, in_specs=in_specs, out_specs=cols, check_vma=False)
```

profile of v0, /device:TPU:16, one launch (start us, length us, event | category | flops | bytes accessed | tf_op | source)
XLA Modules:
  0.0 228.7 jit_solution(13369882979731693289)
XLA Ops:
  0.0 0.7 tile.28
  0.7 0.1 tile.29
  0.8 0.7 tile.30
  1.4 0.1 tile.31
  1.5 0.7 tile.32
  2.2 0.1 tile.33
  2.3 0.7 tile.34
  2.9 0.1 tile.70
  3.0 0.7 tile.71
  3.7 0.1 tile.72
  3.8 0.7 tile.73
  4.4 0.1 tile.74
  4.5 0.0 copy-start.1
  4.6 1.9 copy.26
  6.5 1.3 copy.27
  7.8 0.1 convert_element_type.27
  7.9 0.0 copy-start.6
  7.9 1.3 copy.28
  9.4 0.9 pad_maximum_fusion.refs_6_
  10.3 0.9 copy.24
  11.2 0.8 copy.25
  12.0 0.6 pad_maximum_fusion.1.refs_1_
  12.6 214.2 %layer.1 = bf16[384,512]{1,0:T(8,128)(2,1)} custom-call(bf16[384,512]{1,0:T(8,128)(2,1)} %bitcast.20, f32[2,2048]{1,0:T(2,128)} %pad_maximum_fusion.1.refs_1_, f32[1,4096]{1,0:T(1,128)} %bitcast.23, f32[384,256]{1,0:T(8,128)} %constant.68.clone.refs_3_, f32[384,256]{1,0:T(8,128)} %constant.69.clone.refs_4_, f32[4]{0:T(128)} %refs_5_.1, ...), custom_call_target="tpu_custom_call" | custom-call | tf_op jit(solution)/shard_map/layer/pallas_call | solution.py:375
  226.8 1.9 copy.29
  (34 shorter events, 0.2 us)
Async XLA Ops:
  0.0 4.5 %copy-start = (f32[256]{0:T(256)S(1)}, f32[256]{0:T(256)}, u32[]{:S(2)}) copy-start(f32[256]{0:T(256)} %param.35) | copy-start | bytes 3076
  4.5 3.2 %copy-start.8 = (f32[4096]{0:T(1024)}, f32[4096]{0:T(1024)S(1)}, u32[]{:S(2)}) copy-start(f32[4096]{0:T(1024)S(1)} %select_dynamic-update-slice_fusion) | copy-start | bytes 49156
  4.5 3.2 %copy-start.1 = (f32[2048,256]{1,0:T(8,128)S(1)}, f32[2048,256]{1,0:T(8,128)}, u32[]{:S(2)}) copy-start(f32[2048,256]{1,0:T(8,128)} %param.29) | copy-start | bytes 6291460
  7.8 1.5 copy-start.3
  7.9 1.4 copy-start.4
  7.9 1.4 copy-start.5
  7.9 1.5 copy-start.6
  7.9 2.3 %copy-start.2 = (bf16[512,384]{1,0:T(8,128)(2,1)S(1)}, bf16[512,384]{1,0:T(8,128)(2,1)}, u32[]{:S(2)}) copy-start(bf16[512,384]{1,0:T(8,128)(2,1)} %param.20) | copy-start | bytes 1179652
  9.3 2.0 copy-start.7
  9.3 2.7 %copy-start.9 = (f32[2048]{0:T(1024)S(1)}, f32[2048]{0:T(1024)}, u32[]{:S(2)}) copy-start(f32[2048]{0:T(1024)} %param.22) | copy-start | bytes 24580
  9.3 2.7 %copy-start.10 = (f32[2048]{0:T(1024)S(1)}, f32[2048]{0:T(1024)}, u32[]{:S(2)}) copy-start(f32[2048]{0:T(1024)} %param.21) | copy-start | bytes 24580
where the time goes:
time: 229 us
  Pallas kernels  214 us (93%)
  local copies, waits for them, and re-layouts  12.6 us (6%)
    pallas_call x1, Pallas kernels, on_device(): pl.pallas_call(functools.partial(kernel, (Z, X, Y, C, G, heads)), out_sha...  214 us

commit v1 on v0

--- a/solution.py
+++ b/solution.py
@@ -326,7 +326,7 @@
     if n_tp % C:
         C = 1
     Y = n_tp // C
-    G = 2 if Z % 2 == 0 else Z
+    G = next(g for g in (4, 2, Z) if Z % g == 0)
 
     def on_device(tokens, mix_gain, mlp_gain, wq, wk, wv, wg, wo, wu, wd, sq, sk, sv, sg, so, su, sd, forget):
         width, length = tokens.shape

time: 229 us -> 239 us (1.044)
  the two profiles are of different devices: /device:TPU:16 before, /device:TPU:0 now
where the time goes in v1:
time: 239 us
  Pallas kernels  225 us (94%)
  local copies, waits for them, and re-layouts  12.6 us (5%)
    pallas_call x1, Pallas kernels, on_device(): pl.pallas_call(functools.partial(kernel, (Z, X, Y, C, G, heads)), out_sha...  225 us

profile of v1, /device:TPU:0, one launch (start us, length us, event | category | flops | bytes accessed | tf_op | source)
XLA Modules:
  0.0 239.1 jit_solution(10885766578554990189)
XLA Ops:
  0.0 0.7 tile.28
  0.7 0.1 tile.29
  0.8 0.7 tile.30
  1.4 0.1 tile.31
  1.5 0.7 tile.32
  2.2 0.1 tile.33
  2.3 0.7 tile.34
  2.9 0.1 tile.70
  3.0 0.7 tile.71
  3.7 0.1 tile.72
  3.8 0.7 tile.73
  4.4 0.1 tile.74
  4.5 0.0 copy-start.1
  4.6 1.9 copy.26
  6.5 1.3 copy.27
  7.8 0.1 convert_element_type.27
  7.9 0.0 copy-start.4
  8.0 1.3 copy.28
  9.4 0.9 pad_maximum_fusion.refs_6_
  10.3 0.9 copy.24
  11.2 0.8 copy.25
  12.0 0.6 pad_maximum_fusion.1.refs_1_
  12.6 224.6 %layer.1 = bf16[384,512]{1,0:T(8,128)(2,1)} custom-call(bf16[384,512]{1,0:T(8,128)(2,1)} %bitcast.20, f32[2,2048]{1,0:T(2,128)} %pad_maximum_fusion.1.refs_1_, f32[1,4096]{1,0:T(1,128)} %bitcast.23, f32[384,256]{1,0:T(8,128)} %constant.68.clone.refs_3_, f32[384,256]{1,0:T(8,128)} %constant.69.clone.refs_4_, f32[4]{0:T(128)} %refs_5_.1, ...), custom_call_target="tpu_custom_call" | custom-call | tf_op jit(solution)/shard_map/layer/pallas_call | solution.py:375
  237.2 1.9 copy.29
  (34 shorter events, 0.2 us)
Async XLA Ops:
  0.0 4.5 %copy-start = (f32[256]{0:T(256)S(1)}, f32[256]{0:T(256)}, u32[]{:S(2)}) copy-start(f32[256]{0:T(256)} %param.35) | copy-start | bytes 3076
  4.5 3.3 %copy-start.8 = (f32[4096]{0:T(1024)}, f32[4096]{0:T(1024)S(1)}, u32[]{:S(2)}) copy-start(f32[4096]{0:T(1024)S(1)} %select_dynamic-update-slice_fusion) | copy-start | bytes 49156
  4.5 3.2 %copy-start.1 = (f32[2048,256]{1,0:T(8,128)S(1)}, f32[2048,256]{1,0:T(8,128)}, u32[]{:S(2)}) copy-start(f32[2048,256]{1,0:T(8,128)} %param.29) | copy-start | bytes 6291460
  7.8 1.5 copy-start.3
  7.9 1.4 copy-start.4
  7.9 1.4 copy-start.5
  7.9 1.5 copy-start.6
  7.9 2.4 copy-start.2
  9.3 2.0 copy-start.7
  9.3 2.7 %copy-start.9 = (f32[2048]{0:T(1024)S(1)}, f32[2048]{0:T(1024)}, u32[]{:S(2)}) copy-start(f32[2048]{0:T(1024)} %param.22) | copy-start | bytes 24580
  9.3 2.7 %copy-start.10 = (f32[2048]{0:T(1024)S(1)}, f32[2048]{0:T(1024)}, u32[]{:S(2)}) copy-start(f32[2048]{0:T(1024)} %param.21) | copy-start | bytes 24580

commit v2 on v1

v2 whole, which is shorter than its diff:
```python
import functools

import jax
import jax.numpy as jnp
import numpy as np
from jax import lax
from jax.experimental import pallas as pl
from jax.experimental.pallas import tpu as pltpu
from jax.sharding import PartitionSpec as P

MESH = pl.DeviceIdType.MESH
BF = jnp.bfloat16
F32 = jnp.float32
LANES = 128


def nn(a, b):
    return lax.dot_general(a, b, (((1,), (0,)), ((), ())), preferred_element_type=F32)


def pick(table, at):
    value = jnp.int32(table[0])
    for a in range(1, len(table)):
        value = jnp.where(at == a, jnp.int32(table[a]), value)
    return value


def part_of(n):
    return min(n, LANES)


def scale_rows(s):
    n = s.shape[0]
    if n < LANES:
        return jnp.pad(s, (0, LANES - n))[None, :]
    return s.reshape(-1, LANES)


class Cfg:
    pass


def kernel(cfg, *refs):
    Z, X, Y, C, G = cfg.Z, cfg.X, cfg.Y, cfg.C, cfg.G
    n_tp, n_fs = Y * C, Z * X
    n_dev = n_tp * n_fs
    L, width, D, ret, hw, chunk, rows = cfg.L, cfg.width, cfg.D, cfg.ret, cfg.hw, cfg.chunk, cfg.rows
    head = cfg.head
    (tokens, gains, scales, cos_t, sin_t, forget, wq, wk, wv, wg, wo, wu, wd, out_ref) = refs[:14]
    (tok_g, mix_g, out_full, f_proj, f_up, f_down, o_proj, o_up, o_down, o_out, st_proj, st_out, st_up, st_down,
     parts, core_in, y_out, y_in, z_out, z_in, after, normed, hidden, keep, gain_c, out_c, up_c, down_c, proj_c,
     decay, scale_g, load_sem, local_sem, sc_s, sc_r, wzs, wzr, wxs, wxr,
     t_zs, t_zr, t_ys, t_yr, t_cs, t_cr, m_zs, m_zr, m_ys, m_yr, m_cs, m_cr,
     p_zs, p_zr, p_ys, p_yr, p_xs, p_xr, p_cs, p_cr, rcs, rcr, rys, ryr, rzs, rzr) = refs[14:]
    me = lax.axis_index("fs")
    tp = lax.axis_index("tp")
    z = me // X
    x = lax.rem(me, X)
    y = tp // C
    core = lax.rem(tp, C)
    flat = tp * n_fs + me
    g = lax.rem(z, G)
    base = z - g
    full = [f_proj, f_up, f_down]
    own = [o_proj, o_up, o_down]

    def to_z(zz):
        return {"fs": zz * X + x}

    def to_x(o):
        return {"fs": z * X + lax.rem(x + o, X)}

    def to_y(o):
        return {"tp": lax.rem(y + o, Y) * C + core}

    def to_core(o):
        return {"tp": y * C + lax.rem(core + o, C)}

    def peer(o):
        q = lax.rem(flat + o, n_dev)
        return {"fs": lax.rem(q, n_fs), "tp": q // n_fs}

    barrier = pltpu.get_barrier_semaphore()

    def greet(o, carry):
        pl.semaphore_signal(barrier, inc=1, device_id=peer(o), device_id_type=MESH)
        return carry

    lax.fori_loop(1, n_dev, greet, 0)

    def rows_of(i, n):
        return pl.ds(pl.multiple_of(i * n, n), n)

    own_tok = tok_g.at[g, rows_of(tp, width)]
    loads = [(tokens, own_tok)]
    loads += [(w, st_proj.at[i]) for i, w in enumerate((wq, wk, wv, wg))]
    loads += [(wo, st_out), (wu, st_up), (wd, st_down)]
    loads = [pltpu.make_async_copy(a, b, load_sem.at[i]) for i, (a, b) in enumerate(loads)]
    for copy in loads:
        copy.start()

    pending = []

    def remote(src, dst, ss, rs, where):
        return pltpu.make_async_remote_copy(
            src_ref=src, dst_ref=dst, send_sem=ss, recv_sem=rs, device_id=where, device_id_type=MESH
        )

    def send(*a, when=None):
        copy = remote(*a)
        if when is None:
            copy.start()
        else:
            pl.when(when)(copy.start)
        pending.append((copy, when))

    def arrived(ref, ss, rs):
        remote(ref, ref, ss, rs, to_core(1) if C > 1 else to_z(z)).wait_recv()

    class Spread:
        def __init__(self, n, at, first, ref, zs, zr, ys, yr, cs, cr, xs=None, xr=None):
            self.n, self.at, self.first, self.ref = n, at, first, ref
            self.zs, self.zr, self.ys, self.yr, self.cs, self.cr, self.xs, self.xr = zs, zr, ys, yr, cs, cr, xs, xr
            self.nx = X if xs is not None else 1

        def order(self, i):
            n = self.n
            return pick([sorted(range(n), key=lambda q: (abs(q - a), q))[i] for a in range(n)], self.at)

        def block(self, i, j, k, o):
            tps = lax.rem(y + Y - j, Y) * C + lax.rem(core + C - o, C)
            return self.ref(self.order(i), lax.rem(x + X - k, X), tps)

        def fan_y(self, i):
            piece = self.block(i, 0, 0, 0)
            for j in range(1, Y):
                send(piece, piece, self.ys.at[i, j - 1], self.yr.at[i, j - 1], to_y(j))

        def fan_x(self, i, j):
            piece = self.block(i, j, 0, 0)
            for k in range(1, self.nx):
                send(piece, piece, self.xs.at[i, j, k - 1], self.xr.at[i, j, k - 1], to_x(k))

        def fan_c(self, i, j, k):
            piece = self.block(i, j, k, 0)
            for o in range(1, C):
                send(piece, piece, self.cs.at[i, j, k, o - 1], self.cr.at[i, j, k, o - 1], to_core(o))

        def fan(self, i):
            self.fan_y(i)
            self.fan_x(i, 0)
            self.fan_c(i, 0, 0)

        def start(self):
            piece = self.block(0, 0, 0, 0)
            slot = self.zr.at[self.at]
            send(piece, piece, self.zs.at[0], slot, to_z(self.first + self.at + 1), when=self.at < self.n - 1)
            send(piece, piece, self.zs.at[self.n], slot, to_z(self.first + self.at - 1), when=self.at > 0)
            self.fan(0)

        def on_z(self, i):
            o = self.order(i)
            piece = self.block(i, 0, 0, 0)
            arrived(piece, self.zs.at[i], self.zr.at[o])
            nxt = jnp.where(o < self.at, self.at + 1, self.at - 1)
            send(piece, piece, self.zs.at[i], self.zr.at[o], to_z(self.first + nxt),
                 when=(nxt >= 0) & (nxt < self.n))
            self.fan(i)

        def on_y(self, i):
            for j in range(1, Y):
                arrived(self.block(i, j, 0, 0), self.ys.at[i, j - 1], self.yr.at[i, j - 1])
                self.fan_x(i, j)
                self.fan_c(i, j, 0)

        def on_x(self, i):
            for j in range(Y):
                for k in range(1, self.nx):
                    arrived(self.block(i, j, k, 0), self.xs.at[i, j, k - 1], self.xr.at[i, j, k - 1])
                    self.fan_c(i, j, k)

        def on_c(self, i):
            for j in range(Y):
                for k in range(self.nx):
                    for o in range(1, C):
                        arrived(self.block(i, j, k, o), self.cs.at[i, j, k, o - 1], self.cr.at[i, j, k, o - 1])

    tok = Spread(G, g, base, lambda zi, xi, t: tok_g.at[zi, rows_of(t, width)], t_zs, t_zr, t_ys, t_yr, t_cs, t_cr)
    mix = Spread(G, g, base, lambda zi, xi, t: mix_g.at[:, pl.ds(pl.multiple_of(t * ret + zi * hw, hw), hw)],
                 m_zs, m_zr, m_ys, m_yr, m_cs, m_cr)
    prj = Spread(Z, z, 0, lambda zi, xi, t: out_full.at[rows_of(zi * X + xi, rows), rows_of(t, ret)],
                 p_zs, p_zr, p_ys, p_yr, p_cs, p_cr, p_xs, p_xr)

    def place(w, owner):
        if w == 2:
            return full[w].at[rows_of(owner, rows)]
        if rows % LANES:
            return full[w].at[owner]
        return full[w].at[:, rows_of(owner, rows)]

    def mul(w, here, v):
        if rows % LANES:
            total = nn(full[w][0, here, :], v[0:rows, :])
            for f in range(1, n_fs):
                total += nn(full[w][f, here, :], v[f * rows : (f + 1) * rows, :])
            return total
        return nn(full[w][here, :], v[...])

    def z_send(w):
        for o in range(1, Z):
            to = lax.rem(z + o, Z)
            send(own[w].at[lax.rem(to, G)], place(w, me), wzs.at[w, o - 1], wzr.at[w, o - 1], to_z(to))

    def x_own(w):
        for o in range(1, X):
            send(own[w].at[g], place(w, me), wxs.at[w, 0, o - 1], wxr.at[w, 0, o - 1], to_x(o))
        copy = pltpu.make_async_copy(own[w].at[g], place(w, me), local_sem.at[w])
        copy.start()
        return copy

    def relay(w):
        for k in range(1, Z):
            piece = place(w, lax.rem(z + Z - k, Z) * X + x)
            arrived(piece, wzs.at[w, k - 1], wzr.at[w, k - 1])
            for o in range(1, X):
                send(piece, piece, wxs.at[w, k, o - 1], wxr.at[w, k, o - 1], to_x(o))

    def finish(w, local):
        local.wait()
        for k in range(Z):
            for o in range(1, X):
                owner = lax.rem(z + Z - k, Z) * X + lax.rem(x + X - o, X)
                arrived(place(w, owner), wxs.at[w, k, o - 1], wxr.at[w, k, o - 1])

    def wide(col, n):
        return jnp.concatenate([col] * (n // LANES), axis=1) if n > LANES else col[:, :n]

    def column(row):
        return jnp.broadcast_to(row, (LANES, LANES)).T

    def columns(dst, row, n, count, first):
        w = part_of(n)
        per = n // w

        def one(f, carry):
            for r in range(per):
                c = column(scale_g[first + f, row + r : row + r + 1, :])[:w]
                if w % 8 == 0:
                    dst[pl.ds(pl.multiple_of((f * per + r) * w, 8), w), :] = c
                else:
                    dst[f * w : (f + 1) * w, :] = c
            return carry

        if w % 8 == 0:
            lax.fori_loop(0, count, one, 0)
        else:
            for f in range(count):
                one(f, 0)

    loads[0].wait()
    scale_g[flat] = scales[...]
    pl.semaphore_wait(barrier, n_dev - 1)

    with jax.named_scope("start"):
        tok.start()

        def tell(o, carry):
            remote(scales, scale_g.at[flat], sc_s.at[o], sc_r.at[o], peer(o)).start()
            return carry

        lax.fori_loop(1, n_dev, tell, 0)

    with jax.named_scope("cast"):
        for i in range(4):
            loads[1 + i].wait()
            t = st_proj[i].T
            for k in range(G):
                o_proj[k, i * hw : (i + 1) * hw, :] = t[k * hw : (k + 1) * hw, :].astype(BF)
        z_send(0)
        local0 = x_own(0)
        loads[5].wait()
        own_out = out_full.at[rows_of(me, rows), rows_of(tp, ret)]
        o_out[...] = st_out[...].T.astype(BF)
        copy = pltpu.make_async_copy(o_out, own_out, local_sem.at[3])
        copy.start()
        copy.wait()
        loads[6].wait()
        loads[7].wait()
        step = min(chunk, 512)

        def cast_up(k, carry):
            here = rows_of(k, step)
            o_up[k * step // chunk, pl.ds(pl.multiple_of(lax.rem(k * step, chunk), step), step), :] = (
                st_up[:, here].T.astype(BF))
            o_down[k * step // chunk, :, pl.ds(pl.multiple_of(lax.rem(k * step, chunk), step), step)] = (
                st_down[here, :].T.astype(BF))
            return carry

        lax.fori_loop(0, G * chunk // step, cast_up, 0)

    with jax.named_scope("tables"):
        def gain_row(i, carry):
            gain_c[rows_of(i, LANES), :] = column(gains[pl.ds(i, 1), :])
            return carry

        lax.fori_loop(0, 2 * D // LANES, gain_row, 0)
        krow = lax.broadcasted_iota(jnp.int32, (L, L), 0)
        qcol = lax.broadcasted_iota(jnp.int32, (L, L), 1)
        dist = (qcol - krow).astype(F32)
        for h in range(hw // head):
            rate = forget[g * (hw // head) + h]
            decay[h] = jnp.where(dist >= 0.0, jnp.exp(-rate * jnp.maximum(dist, 0.0)), 0.0)

    with jax.named_scope("tok1"):
        tok.on_z(1)
        tok.on_y(0)
    with jax.named_scope("prj0"):
        prj.start()
    with jax.named_scope("relay0"):
        relay(0)
    for i in range(2, G):
        with jax.named_scope("tok%d" % i):
            tok.on_z(i)
            tok.on_y(i - 1)
    with jax.named_scope("scales"):
        def heard(o, carry):
            slot = scale_g.at[lax.rem(flat + n_dev - o, n_dev)]
            arrived(slot, sc_s.at[o], sc_r.at[o])
            return carry

        lax.fori_loop(1, n_dev, heard, 0)
        for i in range(4):
            columns(proj_c.at[i], i, ret // n_fs, n_fs, tp * n_fs)
        columns(out_c, 4, D // n_dev, n_dev, 0)
        columns(down_c, 5, width // n_fs, n_fs, tp * n_fs)
        columns(up_c, 6, G * chunk // n_fs, n_fs, tp * n_fs)

    with jax.named_scope("finish0"):
        finish(0, local0)
    z_send(1)
    local1 = x_own(1)

    tile = 256 if D % 256 == 0 else D
    r64 = lax.broadcasted_iota(jnp.int32, (head, head), 0)
    c64 = lax.broadcasted_iota(jnp.int32, (head, head), 1)
    odd = lax.rem(r64, 2) == 1
    swap = jnp.where((c64 == r64 - 1) & odd, 1.0, jnp.where((c64 == r64 + 1) & ~odd, -1.0, 0.0)).astype(BF)

    def scaled(src, square, gain_at):
        factor = lax.rsqrt(square / D + 1e-6)

        def one(t, carry):
            here = rows_of(t, tile)
            gain = wide(gain_c[pl.ds(pl.multiple_of(gain_at + t * tile, tile), tile), :], L)
            normed[here, :] = (src[here, :].astype(F32) * factor * gain).astype(BF)
            return carry

        lax.fori_loop(0, D // tile, one, 0)

    def turn(field):
        return field.astype(F32) * cos_t[...] + nn(swap, field) * sin_t[...]

    def attend(i):
        s = tok.order(i)
        src = tok_g.at[s]

        def add(t, square):
            v = src[rows_of(t, tile), :].astype(F32)
            return square + jnp.sum(v * v, axis=0, keepdims=True)

        scaled(src, lax.fori_loop(0, D // tile, add, jnp.zeros((1, L), F32)), 0)
        proj = mul(0, slice(0, 4 * hw), normed)
        heads_at = pl.ds(pl.multiple_of(g * hw, hw), hw)
        q, k, v, gate = [
            (proj[n * hw : (n + 1) * hw, :] * wide(proj_c[n, heads_at, :], L)).astype(BF) for n in range(4)
        ]
        for h in range(hw // head):
            at = slice(h * head, (h + 1) * head)
            rot_q = turn(q[at]).astype(BF)
            rot_k = (turn(k[at]) * head ** (-0.5)).T.astype(BF)
            inner = (nn(rot_k, rot_q) * decay[h]).astype(BF)
            total = nn(v[at], inner)
            mean = jnp.sum(total * total, axis=0, keepdims=True) / head
            f = gate[at].astype(F32)
            value = f / (1.0 + jnp.exp(-f)) * (total * lax.rsqrt(mean + 0.01))
            mix_g[s, pl.ds(pl.multiple_of(tp * ret + g * hw + h * head, head), head), :] = value.astype(BF)

    for i in range(G):
        with jax.named_scope("att%d" % i):
            if i == G - 1:
                tok.on_y(i)
            tok.on_c(i)
            attend(i)
            if i == 0:
                for k in range(1, Z):
                    prj.on_z(k)
    with jax.named_scope("mix_start"):
        mix.start()
    with jax.named_scope("prj_y"):
        for k in range(Z):
            prj.on_y(k)
    with jax.named_scope("relay1"):
        relay(1)
    with jax.named_scope("mix_z"):
        for i in range(1, G):
            mix.on_z(i)
    z_send(2)
    local2 = x_own(2)
    with jax.named_scope("prj_x"):
        for k in range(Z):
            prj.on_x(k)
    with jax.named_scope("mix_y"):
        for i in range(G):
            mix.on_y(i)
    with jax.named_scope("prj_c"):
        for k in range(Z):
            prj.on_c(k)
    with jax.named_scope("finish1"):
        finish(1, local1)
    with jax.named_scope("mix_c"):
        for i in range(G):
            mix.on_c(i)

    def expand(i):
        s = tok.order(i)

        def mixed(t, square):
            here = rows_of(t, tile)
            v = nn(out_full[here, :], mix_g[s]) * wide(out_c[here, :], L)
            a = (tok_g[s, here, :].astype(F32) + v).astype(BF)
            after[here, :] = a
            a = a.astype(F32)
            return square + jnp.sum(a * a, axis=0, keepdims=True)

        scaled(after, lax.fori_loop(0, D // tile, mixed, jnp.zeros((1, L), F32)), D)
        if i == 0:
            keep[...] = after[rows_of(tp, width), :]
        ut = 256 if chunk % 256 == 0 else chunk

        def units(t, carry):
            here = rows_of(t, ut)
            sc = wide(up_c[pl.ds(pl.multiple_of(g * chunk + t * ut, ut), ut), :], L)
            u = jnp.maximum(mul(1, here, normed) * sc, 0.0)
            hidden[i, here, :] = (u * u).astype(BF)
            return carry

        lax.fori_loop(0, chunk // ut, units, 0)

    def block_rows(j, c):
        return rows_of(j * C + c, width)

    def shrink(i):
        def one(t, carry):
            here = rows_of(t, tile)
            parts[i, here, :] = nn(full[2][here, :], hidden[i]).astype(BF)
            return carry

        lax.fori_loop(0, D // tile, one, 0)
        for o in range(1, C):
            for j in range(Y):
                send(parts.at[i, block_rows(j, lax.rem(core + o, C))], core_in.at[i, o - 1, j],
                     rcs.at[i, o - 1, j], rcr.at[i, o - 1, j], to_core(o))

    def reduce_core(i):
        for o in range(1, C):
            for j in range(Y):
                arrived(core_in.at[i, o - 1, j], rcs.at[i, o - 1, j], rcr.at[i, o - 1, j])
        for j in range(Y):
            value = parts[i, block_rows(j, core), :].astype(F32)
            for o in range(1, C):
                value += core_in[i, o - 1, j].astype(F32)
            y_out[i, j] = value.astype(BF)
        for j in range(1, Y):
            send(y_out.at[i, lax.rem(y + j, Y)], y_in.at[i, j - 1], rys.at[i, j - 1], ryr.at[i, j - 1], to_y(j))

    def reduce_y(i):
        value = y_out[i, y].astype(F32)
        for j in range(1, Y):
            arrived(y_in.at[i, j - 1], rys.at[i, j - 1], ryr.at[i, j - 1])
            value += y_in[i, j - 1].astype(F32)
        if i:
            z_out[i] = value.astype(BF)
            send(z_out.at[i], z_in.at[g], rzs.at[i], rzr.at[g], to_z(base + tok.order(i)))
        return value

    order = list(range(G - 1, -1, -1))
    for i in order[::-1]:
        with jax.named_scope("expand%d" % i):
            expand(i)
            if i == 0:
                relay(2)
    with jax.named_scope("finish2"):
        finish(2, local2)
    for n, i in enumerate(order):
        with jax.named_scope("shrink%d" % i):
            shrink(i)
            if n:
                reduce_core(order[n - 1])
    with jax.named_scope("reduce"):
        reduce_core(order[-1])
        for i in order:
            total = reduce_y(i)
    with jax.named_scope("final"):
        for i in range(1, G):
            o = tok.order(i)
            arrived(z_in.at[o], rzs.at[i], rzr.at[o])
            total += z_in[o].astype(F32)
        out_ref[...] = (keep[...].astype(F32) + total * wide(down_c[...], L)).astype(BF)
    for copy, when in pending:
        if when is None:
            copy.wait_send()
        else:
            pl.when(when)(copy.wait_send)

    def told(o, carry):
        remote(scales, scale_g.at[flat], sc_s.at[o], sc_r.at[o], peer(o)).wait_send()
        return carry

    lax.fori_loop(1, n_dev, told, 0)


def tables(length, head):
    half = head // 2
    inverse = 1.0 / 10000.0 ** np.linspace(0.0, 1.0, half)
    angle = np.arange(length)[:, None] * inverse.astype(np.float32).astype(np.float64)[None, :]
    spread = lambda a: np.repeat(a, 2, axis=1).T.astype(np.float32)
    return spread(np.cos(angle)), spread(np.sin(angle))


def solution(mesh):
    n_fs, n_tp = mesh.shape["fs"], mesh.shape["tp"]
    heights = [getattr(d, "coords", (0, 0, i))[2] for i, d in enumerate(mesh.devices[:, 0])]
    X = heights.count(heights[0])
    if n_fs % X:
        X = 1
    Z = n_fs // X
    cores = [getattr(d, "core_on_chip", 0) for d in mesh.devices[0]]
    C = len(set(cores))
    if n_tp % C:
        C = 1
    Y = n_tp // C

    def on_device(tokens, mix_gain, mlp_gain, wq, wk, wv, wg, wo, wu, wd, sq, sk, sv, sg, so, su, sd, forget):
        cfg = Cfg()
        cfg.Z, cfg.X, cfg.Y, cfg.C = Z, X, Y, C
        width, L = tokens.shape
        cfg.width, cfg.L, cfg.D = width, L, width * n_tp
        D = cfg.D
        heads = forget.shape[0]
        G = cfg.G = next(q for q in (4, 2, 1) if Z % q == 0 and heads % q == 0)
        ret = cfg.ret = wq.shape[1]
        cfg.head = ret // heads
        hw = cfg.hw = ret // G
        chunk = cfg.chunk = wu.shape[1] // G
        rows = cfg.rows = wq.shape[0]
        n_dev = n_fs * n_tp
        scales = jnp.concatenate([scale_rows(s) for s in (sq, sk, sv, sg, so, sd, su)])
        scales = jnp.pad(scales, ((0, -scales.shape[0] % 8), (0, 0)))
        gains = jnp.concatenate([mix_gain, mlp_gain]).reshape(-1, LANES)
        cos_t, sin_t = tables(L, cfg.head)
        vm = pl.BlockSpec(memory_space=pltpu.VMEM)
        hbm = pl.BlockSpec(memory_space=pl.ANY)
        dma = pltpu.SemaphoreType.DMA
        strided = rows % LANES == 0
        vmem = lambda *shape, t=BF: pltpu.VMEM(shape, t)
        stack = (lambda n: vmem(n, D)) if strided else (lambda n: vmem(n_fs, n, rows))
        scratch = [
            vmem(G, D, L), vmem(G, ret * n_tp, L), vmem(D, ret * n_tp), stack(4 * hw), stack(chunk), vmem(D, chunk),
            vmem(G, 4 * hw, rows), vmem(G, chunk, rows), vmem(G, rows, chunk), vmem(rows, ret),
            vmem(4, rows, ret, t=F32), vmem(*wo.shape, t=F32), vmem(*wu.shape, t=F32), vmem(*wd.shape, t=F32),
            vmem(G, D, L), vmem(G, max(C - 1, 1), Y, width, L), vmem(G, Y, width, L),
            vmem(G, max(Y - 1, 1), width, L), vmem(G, width, L), vmem(G, width, L),
            vmem(D, L), vmem(D, L), vmem(G, chunk, L), vmem(width, L),
            vmem(2 * D, LANES, t=F32), vmem(D, LANES, t=F32), vmem(G * chunk, LANES, t=F32),
            vmem(width, LANES, t=F32), vmem(4, ret, LANES, t=F32), vmem(hw // cfg.head, L, L, t=F32),
            vmem(n_dev, *scales.shape, t=F32), dma((8,)), dma((4,)),
        ]
        line = lambda n, nx: [(n + 1,), (n,), (n, Y), (n, Y), (n, Y, nx, C), (n, Y, nx, C)]
        shapes = [(n_dev,), (n_dev,), (3, Z), (3, Z), (3, Z, X), (3, Z, X)] + line(G, 1) + line(G, 1)
        first = line(Z, X)
        shapes += first[:4] + [(Z, Y, X), (Z, Y, X)] + first[4:]
        shapes += [(G, C, Y), (G, C, Y), (G, Y), (G, Y), (G,), (G,)]
        scratch += [dma(s) for s in shapes]
        return pl.pallas_call(
            functools.partial(kernel, cfg),
            out_shape=jax.ShapeDtypeStruct((width, L), BF),
            in_specs=[hbm] + [vm] * 4 + [pl.BlockSpec(memory_space=pltpu.SMEM)] + [hbm] * 7,
            out_specs=vm,
            scratch_shapes=scratch,
            compiler_params=pltpu.CompilerParams(
                collective_id=0, has_side_effects=True, vmem_limit_bytes=60 * 2**20
            ),
            name="layer",
        )(tokens, gains, scales, jnp.asarray(cos_t), jnp.asarray(sin_t), forget, wq, wk, wv, wg, wo, wu, wd)

    cut = P(("tp", "fs"))
    rows, cols = P("fs", "tp"), P("tp", "fs")
    in_specs = (cols, P(), P(), rows, rows, rows, rows, cols, rows, cols) + (cut,) * 7 + (P("tp"),)
    return jax.shard_map(on_device, mesh=mesh, in_specs=in_specs, out_specs=cols, check_vma=False)
```

time: 239 us -> 201 us (0.84)
  the two profiles are of different devices: /device:TPU:0 before, /device:TPU:16 now
where the time goes in v2:
time: 201 us; the launch traced here: 198 us
  Pallas kernels  191 us (95%)
  local copies, waits for them, and re-layouts  5.09 us (3%)
    pallas_call x1, Pallas kernels, on_device(): pl.pallas_call(functools.partial(kernel, cfg), out_shape=jax.ShapeDtypeSt...  191 us

profile of v2, /device:TPU:16, one launch (start us, length us, event | category | flops | bytes accessed | tf_op | source)
XLA Modules:
  0.0 197.7 jit_solution(5703073290440867451)
XLA Ops:
  0.0 0.7 pad_bitcast_fusion.4
  0.7 0.7 pad_bitcast_fusion.2
  1.4 0.7 pad_bitcast_fusion
  2.0 1.3 concatenate.14.refs_2_
  3.3 1.3 pad_maximum_fusion.refs_1_
  4.6 191.2 %layer.1 = bf16[512,384]{1,0:T(8,128)(2,1)} custom-call(bf16[512,384]{1,0:T(8,128)(2,1)} %refs_0_.1, f32[32,128]{1,0:T(8,128)} %pad_maximum_fusion.refs_1_, f32[8,128]{1,0:T(8,128)} %concatenate.14.refs_2_, f32[64,384]{1,0:T(8,128)} %constant.7.clone.refs_3_, f32[64,384]{1,0:T(8,128)} %constant.8.clone.refs_4_, f32[4]{0:T(128)} %refs_5_.1, ...), custom_call_target="tpu_custom_call" | custom-call | tf_op jit(solution)/shard_map/layer/pallas_call | solution.py:584
  195.9 1.8 copy.22

commit v3 on v2

v3 whole, which is shorter than its diff:
```python
import functools
import math

import jax
import jax.numpy as jnp
import numpy as np
from jax import lax
from jax.experimental import pallas as pl
from jax.experimental.pallas import tpu as pltpu
from jax.sharding import PartitionSpec as P

MESH = pl.DeviceIdType.MESH
BF = jnp.bfloat16
F32 = jnp.float32
LANES = 128


def nn(a, b):
    return lax.dot_general(a, b, (((1,), (0,)), ((), ())), preferred_element_type=F32)


def pick(table, at):
    value = jnp.int32(table[0])
    for a in range(1, len(table)):
        value = jnp.where(at == a, jnp.int32(table[a]), value)
    return value


def part_of(n):
    return min(n, LANES)


def scale_rows(s):
    n = s.shape[0]
    return s.reshape(-1, part_of(n))


class Cfg:
    pass


def kernel(cfg, *refs):
    Z, X, Y, C, G = cfg.Z, cfg.X, cfg.Y, cfg.C, cfg.G
    n_tp, n_fs = Y * C, Z * X
    n_dev = n_tp * n_fs
    L, width, D, ret, hw, chunk, rows = cfg.L, cfg.width, cfg.D, cfg.ret, cfg.hw, cfg.chunk, cfg.rows
    head, Q, U = cfg.head, cfg.Q, cfg.U
    rq, uh = rows // Q, chunk // U
    DOWN = 1 + U
    (tokens, mix_gain, mlp_gain, cos_t, sin_t, forget, wq, wk, wv, wg, wo, wu, wd) = refs[:13]
    own_scales, out_ref = refs[13:20], refs[20]
    (tok_g, mix_g, out_full, f_proj, f_up, f_down, o_proj, o_up, o_down, o_out, st_proj, st_out, st_up, st_down,
     parts, core_in, y_out, y_in, z_out, z_in, after, normed, hidden, keep, gain_c, out_c, up_c, down_c, proj_c,
     decay, scale_g, load_sem, local_sem, sc_s, sc_r, wzs, wzr, wxs, wxr,
     t_zs, t_zr, t_ys, t_yr, t_cs, t_cr, m_zs, m_zr, m_ys, m_yr, m_cs, m_cr,
     p_zs, p_zr, p_ys, p_yr, p_xs, p_xr, p_cs, p_cr, rcs, rcr, rys, ryr, rzs, rzr, ncs, ncr, scales) = refs[21:]
    me = lax.axis_index("fs")
    tp = lax.axis_index("tp")
    z = me // X
    x = lax.rem(me, X)
    y = tp // C
    core = lax.rem(tp, C)
    flat = tp * n_fs + me
    g = lax.rem(z, G)
    base = z - g
    strided = rows % LANES == 0

    def to_z(zz):
        return {"fs": zz * X + x}

    def to_x(o):
        return {"fs": z * X + lax.rem(x + o, X)}

    def to_y(o):
        return {"tp": lax.rem(y + o, Y) * C + core}

    def to_core(o):
        return {"tp": y * C + lax.rem(core + o, C)}

    def peer(o):
        q = lax.rem(flat + o, n_dev)
        return {"fs": lax.rem(q, n_fs), "tp": q // n_fs}

    barrier = pltpu.get_barrier_semaphore()

    def greet(o, carry):
        pl.semaphore_signal(barrier, inc=1, device_id=peer(o), device_id_type=MESH)
        return carry

    lax.fori_loop(1, n_dev, greet, 0)

    def rows_of(i, n):
        return pl.ds(pl.multiple_of(i * n, n), n)

    def seq_at(s):
        return pl.ds(pl.multiple_of(s * L, LANES), L)

    own_tok = tok_g.at[rows_of(tp, width), seq_at(g)]
    loads = [(tokens, own_tok)]
    loads += [(w, st_proj.at[i]) for i, w in enumerate((wq, wk, wv, wg))]
    loads += [(wo, st_out), (wu, st_up), (wd, st_down)]
    loads = [pltpu.make_async_copy(a, b, load_sem.at[i]) for i, (a, b) in enumerate(loads)]
    for copy in loads:
        copy.start()

    pending = []

    def remote(src, dst, ss, rs, where):
        return pltpu.make_async_remote_copy(
            src_ref=src, dst_ref=dst, send_sem=ss, recv_sem=rs, device_id=where, device_id_type=MESH
        )

    def emit(waits, copies, when=None, track=True):
        def go():
            for copy in waits:
                copy.wait_recv()
            for copy, ok in copies:
                if ok is None:
                    copy.start()
                else:
                    pl.when(ok)(copy.start)

        if when is None:
            go()
        else:
            pl.when(when)(go)
        if track:
            pending.extend(copies)

    def send(*a):
        emit([], [(remote(*a), None)])

    def arrived(ref, ss, rs):
        remote(ref, ref, ss, rs, to_core(1) if C > 1 else to_z(z)).wait_recv()

    class Spread:
        def __init__(self, n, at, first, ref, zs, zr, ys, yr, cs, cr, xs=None, xr=None):
            self.n, self.at, self.first, self.ref = n, at, first, ref
            self.zs, self.zr, self.ys, self.yr, self.cs, self.cr, self.xs, self.xr = zs, zr, ys, yr, cs, cr, xs, xr
            self.nx = X if xs is not None else 1

        def order(self, i):
            n = self.n
            return pick([sorted(range(n), key=lambda q: (abs(q - a), q))[i] for a in range(n)], self.at)

        def block(self, i, j, k, o):
            tps = lax.rem(y + Y - j, Y) * C + lax.rem(core + C - o, C)
            return self.ref(self.order(i), lax.rem(x + X - k, X), tps)

        def fan_y(self, i):
            piece = self.block(i, 0, 0, 0)
            return [(remote(piece, piece, self.ys.at[i, j - 1], self.yr.at[i, j - 1], to_y(j)), None)
                    for j in range(1, Y)]

        def fan_x(self, i, j):
            piece = self.block(i, j, 0, 0)
            return [(remote(piece, piece, self.xs.at[i, j, k - 1], self.xr.at[i, j, k - 1], to_x(k)), None)
                    for k in range(1, self.nx)]

        def fan_c(self, i, j, k):
            piece = self.block(i, j, k, 0)
            return [(remote(piece, piece, self.cs.at[i, j, k, o - 1], self.cr.at[i, j, k, o - 1], to_core(o)), None)
                    for o in range(1, C)]

        def fan(self, i):
            return self.fan_y(i) + self.fan_x(i, 0) + self.fan_c(i, 0, 0)

        def start_z(self, when=None, track=True):
            piece = self.block(0, 0, 0, 0)
            slot = self.zr.at[self.at]
            copies = []
            for sem, step in ((0, 1), (self.n, -1)):
                to = self.at + step
                copies.append((remote(piece, piece, self.zs.at[sem], slot, to_z(self.first + to)),
                               (to >= 0) & (to < self.n)))
            emit([], copies, when, track)

        def start(self):
            self.start_z()
            emit([], self.fan(0))

        def on_z(self, i, when=None, track=True):
            o = self.order(i)
            piece = self.block(i, 0, 0, 0)
            nxt = jnp.where(o < self.at, self.at + 1, self.at - 1)
            copy = remote(piece, piece, self.zs.at[i], self.zr.at[o], to_z(self.first + nxt))
            emit([copy], [(copy, (nxt >= 0) & (nxt < self.n))] + self.fan(i), when, track)

        def on_y(self, i, when=None, track=True):
            for j in range(1, Y):
                piece = self.block(i, j, 0, 0)
                wait = remote(piece, piece, self.ys.at[i, j - 1], self.yr.at[i, j - 1], to_y(j))
                emit([wait], self.fan_x(i, j) + self.fan_c(i, j, 0), when, track)

        def on_x(self, i):
            for j in range(Y):
                for k in range(1, self.nx):
                    arrived(self.block(i, j, k, 0), self.xs.at[i, j, k - 1], self.xr.at[i, j, k - 1])
                    emit([], self.fan_c(i, j, k))

        def on_c(self, i):
            for j in range(Y):
                for k in range(self.nx):
                    for o in range(1, C):
                        arrived(self.block(i, j, k, o), self.cs.at[i, j, k, o - 1], self.cr.at[i, j, k, o - 1])

    tok = Spread(G, g, base, lambda zi, xi, t: tok_g.at[rows_of(t, width), seq_at(zi)], t_zs, t_zr, t_ys, t_yr, t_cs, t_cr)
    mix = Spread(G, g, base, lambda zi, xi, t: mix_g.at[pl.ds(pl.multiple_of(t * ret + zi * hw, hw), hw)],
                 m_zs, m_zr, m_ys, m_yr, m_cs, m_cr)
    prj = Spread(Z, z, 0, lambda zi, xi, t: out_full.at[rows_of(zi * X + xi, rows), rows_of(t, ret)],
                 p_zs, p_zr, p_ys, p_yr, p_cs, p_cr, p_xs, p_xr)

    def place(w, owner):
        if w >= DOWN:
            return f_down.at[w - DOWN, rows_of(owner, rq)]
        ref = f_proj if w == 0 else f_up.at[w - 1]
        return ref.at[:, rows_of(owner, rows)] if strided else ref.at[owner]

    def mine(w, k):
        if w >= DOWN:
            return o_down.at[k, w - DOWN]
        return o_proj.at[k] if w == 0 else o_up.at[k, w - 1]

    def mul(ref, v):
        if strided:
            return nn(ref[...], v)
        total = nn(ref[0], v[0:rows, :])
        for f in range(1, n_fs):
            total += nn(ref[f], v[f * rows : (f + 1) * rows, :])
        return total

    locals_ = {}

    def z_send(w, when=None, track=True):
        copies = []
        for i in range(1, Z):
            to = prj.order(i)
            o = lax.rem(to + Z - z, Z) - 1
            copy = remote(mine(w, lax.rem(to, G)), place(w, me), wzs.at[w, o], wzr.at[w, o], to_z(to))
            copies.append((copy, None))
        emit([], copies, when, track)

    def x_own(w):
        for o in range(1, X):
            send(mine(w, g), place(w, me), wxs.at[w, 0, o - 1], wxr.at[w, 0, o - 1], to_x(o))
        copy = pltpu.make_async_copy(mine(w, g), place(w, me), local_sem.at[w])
        copy.start()
        locals_[w] = copy

    def relay(w, when=None, track=True):
        for k in range(1, Z):
            piece = place(w, lax.rem(z + Z - k, Z) * X + x)
            wait = remote(piece, piece, wzs.at[w, k - 1], wzr.at[w, k - 1], to_x(1) if X > 1 else to_core(1))
            emit([wait], [(remote(piece, piece, wxs.at[w, k, o - 1], wxr.at[w, k, o - 1], to_x(o)), None)
                          for o in range(1, X)], when, track)

    def finish(w):
        locals_[w].wait()
        for k in range(Z):
            for o in range(1, X):
                owner = lax.rem(z + Z - k, Z) * X + lax.rem(x + X - o, X)
                arrived(place(w, owner), wxs.at[w, k, o - 1], wxr.at[w, k, o - 1])

    def wide(col, n):
        return jnp.concatenate([col] * (n // LANES), axis=1) if n > LANES else col[:, :n]

    def column(row):
        return jnp.broadcast_to(row, (LANES, LANES)).T

    def columns(dst, row, n, count, first):
        w = part_of(n)
        per = n // w

        def one(f, carry):
            for r in range(per):
                c = column(scale_g[first + f, row + r : row + r + 1, :])[:w]
                if w % 8 == 0:
                    dst[pl.ds(pl.multiple_of((f * per + r) * w, 8), w), :] = c
                else:
                    dst[f * w : (f + 1) * w, :] = c
            return carry

        if w % 8 == 0:
            lax.fori_loop(0, count, one, 0, unroll=math.gcd(count, 4))
        else:
            for f in range(count):
                one(f, 0)

    loads[0].wait()
    scales[...] = jnp.zeros_like(scales)
    at = 0
    for ref in own_scales:
        n, w = ref.shape
        scales[at : at + n, :w] = ref[...]
        at += n
    scale_g[flat] = scales[...]
    pl.semaphore_wait(barrier, n_dev - 1)

    with jax.named_scope("start"):
        tok.start()

        def tell(o, carry):
            remote(scales, scale_g.at[flat], sc_s.at[o], sc_r.at[o], peer(o)).start()
            return carry

        lax.fori_loop(1, n_dev, tell, 0)

    ends = (z == 0) | (z == Z - 1)
    with jax.named_scope("cast"):
        for i in range(4):
            loads[1 + i].wait()
            t = st_proj[i].T
            for k in range(G):
                o_proj[k, i * hw : (i + 1) * hw, :] = t[k * hw : (k + 1) * hw, :].astype(BF)
        z_send(0, when=ends)
        x_own(0)
        loads[5].wait()
        own_out = out_full.at[rows_of(me, rows), rows_of(tp, ret)]
        o_out[...] = st_out[...].T.astype(BF)
        copy = pltpu.make_async_copy(o_out, own_out, local_sem.at[DOWN + Q])
        copy.start()
        copy.wait()
        prj.start_z(ends)
        loads[6].wait()
        loads[7].wait()

        def cast_up(k, carry):
            at = rows_of(k, chunk)
            t = st_up[:, at].T.astype(BF)
            for i in range(U):
                o_up[k, i] = t[i * uh : (i + 1) * uh]
            t = st_down[at, :].T.astype(BF)
            for i in range(Q):
                o_down[k, i] = t[i * rq : (i + 1) * rq]
            return carry

        lax.fori_loop(0, G, cast_up, 0)
        for w in range(1, DOWN + Q):
            x_own(w)

    with jax.named_scope("tables"):
        def gain_row(i, carry):
            gain_c[0, rows_of(i, LANES), :] = column(mix_gain[pl.ds(i, 1), :])
            gain_c[1, rows_of(i, LANES), :] = column(mlp_gain[pl.ds(i, 1), :])
            return carry

        lax.fori_loop(0, D // LANES, gain_row, 0, unroll=4)
        krow = lax.broadcasted_iota(jnp.int32, (L, L), 0)
        qcol = lax.broadcasted_iota(jnp.int32, (L, L), 1)
        dist = (qcol - krow).astype(F32)
        for h in range(hw // head):
            rate = forget[g * (hw // head) + h]
            decay[h] = jnp.where(dist >= 0.0, jnp.exp(-rate * jnp.maximum(dist, 0.0)), 0.0)

    with jax.named_scope("tok1"):
        tok.on_z(1)
        if G > 2:
            tok.on_z(2)
        z_send(0, when=jnp.logical_not(ends), track=False)
        tok.on_y(0)
    with jax.named_scope("scales"):
        def heard(o, carry):
            slot = scale_g.at[lax.rem(flat + n_dev - o, n_dev)]
            arrived(slot, sc_s.at[o], sc_r.at[o])
            return carry

        lax.fori_loop(1, n_dev, heard, 0)
        for i in range(4):
            columns(proj_c.at[i], i, ret // n_fs, n_fs, tp * n_fs)
    inner = jnp.logical_not(ends)
    with jax.named_scope("tok_y1"):
        tok.on_y(1)
    with jax.named_scope("relay0"):
        relay(0, when=ends)
        for w in range(1, DOWN):
            z_send(w, when=ends)
    with jax.named_scope("tok3"):
        for i in range(3, G):
            tok.on_z(i)
    with jax.named_scope("relay0b"):
        prj.start_z(inner, track=False)
        emit([], prj.fan(0))
        relay(0, when=inner, track=False)
        for k in range(1, min(Z, 3)):
            prj.on_z(k, when=inner)
    with jax.named_scope("finish0"):
        finish(0)

    tile = 256 if D % 256 == 0 else D
    r64 = lax.broadcasted_iota(jnp.int32, (head, head), 0)
    c64 = lax.broadcasted_iota(jnp.int32, (head, head), 1)
    odd = lax.rem(r64, 2) == 1
    swap = jnp.where((c64 == r64 - 1) & odd, 1.0, jnp.where((c64 == r64 + 1) & ~odd, -1.0, 0.0)).astype(BF)

    def turn(field):
        return field.astype(F32) * cos_t[...] + nn(swap, field) * sin_t[...]

    def attend(i):
        at = seq_at(tok.order(i))

        def add(t, square):
            v = tok_g[rows_of(t, tile), at].astype(F32)
            return square + jnp.sum(v * v, axis=0, keepdims=True)

        square = lax.fori_loop(0, D // tile, add, jnp.zeros((1, L), F32))
        factor = lax.rsqrt(square / D + 1e-6)

        def one(t, carry):
            here = rows_of(t, tile)
            normed[here, :] = (tok_g[here, at].astype(F32) * factor * wide(gain_c[0, here, :], L)).astype(BF)
            return carry

        lax.fori_loop(0, D // tile, one, 0)
        proj = mul(f_proj, normed[...])
        heads_at = pl.ds(pl.multiple_of(g * hw, hw), hw)
        q, k, v, gate = [
            (proj[n * hw : (n + 1) * hw, :] * wide(proj_c[n, heads_at, :], L)).astype(BF) for n in range(4)
        ]
        for h in range(hw // head):
            of = slice(h * head, (h + 1) * head)
            rot_q = turn(q[of]).astype(BF)
            rot_k = (turn(k[of]) * head ** (-0.5)).T.astype(BF)
            inner = (nn(rot_k, rot_q) * decay[h]).astype(BF)
            total = nn(v[of], inner)
            mean = jnp.sum(total * total, axis=0, keepdims=True) / head
            f = gate[of].astype(F32)
            value = f / (1.0 + jnp.exp(-f)) * (total * lax.rsqrt(mean + 0.01))
            mix_g[pl.ds(pl.multiple_of(tp * ret + g * hw + h * head, head), head), at] = value.astype(BF)

    with jax.named_scope("tok_y2"):
        for i in range(2, G - 1):
            tok.on_y(i)
    for i in range(G):
        if i == G - 1 and i > 1:
            with jax.named_scope("tok_y3"):
                tok.on_y(i, when=ends, track=False)
        with jax.named_scope("att%d" % i):
            tok.on_c(i)
            attend(i)
        if i == 0 and G > 2:
            with jax.named_scope("tok_y3"):
                tok.on_y(G - 1, when=inner)
        if i == min(1, G - 1):
            with jax.named_scope("prj_z0"):
                for k in range(3, Z):
                    prj.on_z(k, when=inner)
                for w in range(1, 1 + U // 2):
                    z_send(w, when=inner, track=False)
        if i == G - 2:
            with jax.named_scope("prj_y0"):
                prj.on_y(0)
    with jax.named_scope("mix_start"):
        mix.start()
    with jax.named_scope("prj_y12"):
        for k in range(1, min(Z, 3)):
            prj.on_y(k, when=inner)
    with jax.named_scope("prj_z"):
        for k in range(1, min(Z, 3)):
            prj.on_z(k, when=ends, track=False)
        for k in range(3, Z):
            prj.on_z(k, when=ends, track=False)
    with jax.named_scope("mix_z"):
        for i in range(1, min(G, 3)):
            mix.on_z(i)
    with jax.named_scope("prj_y1"):
        for k in range(1, min(Z, 3)):
            prj.on_y(k, when=ends, track=False)
    with jax.named_scope("mix_z3"):
        for i in range(3, G):
            mix.on_z(i)
    for w in range(DOWN, DOWN + Q):
        z_send(w, when=ends)
    with jax.named_scope("prj_y3"):
        for k in range(3, Z):
            prj.on_y(k)
    with jax.named_scope("columns"):
        columns(out_c, 4, D // n_dev, n_dev, 0)
        columns(down_c, 5, width // n_fs, n_fs, tp * n_fs)
        columns(up_c, 6, G * chunk // n_fs, n_fs, tp * n_fs)
    with jax.named_scope("relay1"):
        for w in range(1, 1 + U // 2):
            relay(w)
    with jax.named_scope("mix_y"):
        for i in range(G):
            mix.on_y(i)
            if i == 1:
                for w in range(1 + U // 2, DOWN + Q):
                    z_send(w, when=inner, track=False)
    with jax.named_scope("prj_x"):
        for k in range(Z):
            prj.on_x(k)
    with jax.named_scope("prj_c"):
        for k in range(Z):
            prj.on_c(k)
    with jax.named_scope("mix_c"):
        for i in range(G):
            mix.on_c(i)

    tb = cfg.tb
    n_blocks = G * L // tb

    def settle(n):
        b = n * C + core
        at = rows_of(b, tb)
        v = nn(out_full[...], mix_g[:, at]) * wide(out_c[...], tb)
        a = (tok_g[:, at].astype(F32) + v).astype(BF).astype(F32)
        factor = lax.rsqrt(jnp.sum(a * a, axis=0, keepdims=True) / D + 1e-6)
        after[b] = (a * factor * wide(gain_c[1], tb)).astype(BF)
        for o in range(1, C):
            send(after.at[b], after.at[b], ncs.at[n, o - 1], ncr.at[n, o - 1], to_core(o))

    def settled(n):
        for o in range(1, C):
            arrived(after.at[n * C + lax.rem(core + C - o, C)], ncs.at[n, o - 1], ncr.at[n, o - 1])

    def expand(b, carry):
        at = rows_of(b, tb)
        for i in range(U):
            sc = wide(up_c[pl.ds(pl.multiple_of(g * chunk + i * uh, uh), uh), :], tb)
            u = jnp.maximum(mul(f_up.at[i], after[b]) * sc, 0.0)
            hidden[i * uh : (i + 1) * uh, at] = (u * u).astype(BF)
        return carry

    wt = width // Q
    ppt = n_fs // n_tp

    def shrink(q):
        def one(b, carry):
            at = rows_of(b, tb)
            parts[q, :, at] = nn(f_down[q], hidden[:, at]).astype(BF)
            return carry

        lax.fori_loop(0, G * L // tb, one, 0)
        for o in range(1, C):
            for j in range(Y):
                send(parts.at[q, rows_of(j * C + lax.rem(core + o, C), wt)], core_in.at[q, o - 1, j],
                     rcs.at[q, o - 1, j], rcr.at[q, o - 1, j], to_core(o))

    def reduce_core(q):
        for o in range(1, C):
            for j in range(Y):
                arrived(core_in.at[q, o - 1, j], rcs.at[q, o - 1, j], rcr.at[q, o - 1, j])
        for n in range(Y - 1, -1, -1):
            j = lax.rem(y + n, Y)
            value = parts[q, rows_of(j * C + core, wt), :].astype(F32)
            for o in range(1, C):
                value += core_in[q, o - 1, j].astype(F32)
            y_out[q, j] = value.astype(BF)
            if n:
                send(y_out.at[q, j], y_in.at[q, n - 1], rys.at[q, n - 1], ryr.at[q, n - 1], to_y(n))

    def reduce_y(q):
        value = y_out[q, y].astype(F32)
        for j in range(1, Y):
            arrived(y_in.at[q, j - 1], rys.at[q, j - 1], ryr.at[q, j - 1])
            value += y_in[q, j - 1].astype(F32)
        z_out[q] = value.astype(BF)
        for i in range(G - 1, 0, -1):
            s = tok.order(i)
            send(z_out.at[q, :, seq_at(s)], z_in.at[q, g], rzs.at[q, i], rzr.at[q, g], to_z(base + s))

    def reduce_z(q):
        total = z_out[q, :, seq_at(g)].astype(F32)
        for i in range(1, G):
            o = tok.order(i)
            arrived(z_in.at[q, o], rzs.at[q, i], rzr.at[q, o])
            total += z_in[q, o].astype(F32)
        for h in range(ppt):
            here = slice(h * rows + q * rq, h * rows + (q + 1) * rq)
            t = total[h * rq : (h + 1) * rq] * wide(down_c[here, :], L)
            out_ref[here, :] = (keep[here, :].astype(F32) + t).astype(BF)

    for n in range(n_blocks // C):
        with jax.named_scope("settle%d" % n):
            settle(n)
            if n == 0:
                for w in range(1 + U // 2, DOWN):
                    relay(w)
    with jax.named_scope("keep"):
        mine_at = rows_of(tp, width)
        v = nn(out_full[mine_at, :], mix_g[:, seq_at(g)]) * wide(out_c[mine_at, :], L)
        keep[...] = (tok_g[mine_at, seq_at(g)].astype(F32) + v).astype(BF)
    with jax.named_scope("finish1"):
        for w in range(1, 1 + U):
            finish(w)
    with jax.named_scope("expand"):
        for n in range(n_blocks // C):
            settled(n)
        relay(DOWN)
        lax.fori_loop(0, n_blocks, expand, 0)
    for n in range(Q + 1):
        with jax.named_scope("down%d" % n):
            if n < Q:
                with jax.named_scope("drel"):
                    for w in range(n + 1, Q if n == 1 else n + 2):
                        if w < Q and n < 2:
                            relay(DOWN + w)
                with jax.named_scope("dfin"):
                    finish(DOWN + n)
                with jax.named_scope("shrink"):
                    shrink(n)
                with jax.named_scope("rcore"):
                    reduce_core(n)
            if n:
                with jax.named_scope("ry"):
                    reduce_y(n - 1)
    with jax.named_scope("final"):
        for q in range(Q):
            reduce_z(q)
    for copy, when in pending:
        if when is None:
            copy.wait_send()
        else:
            pl.when(when)(copy.wait_send)

    def told(o, carry):
        remote(scales, scale_g.at[flat], sc_s.at[o], sc_r.at[o], peer(o)).wait_send()
        return carry

    lax.fori_loop(1, n_dev, told, 0)


def tables(length, head):
    half = head // 2
    inverse = 1.0 / 10000.0 ** np.linspace(0.0, 1.0, half)
    angle = np.arange(length)[:, None] * inverse.astype(np.float32).astype(np.float64)[None, :]
    spread = lambda a: np.repeat(a, 2, axis=1).T.astype(np.float32)
    return spread(np.cos(angle)), spread(np.sin(angle))


def solution(mesh):
    n_fs, n_tp = mesh.shape["fs"], mesh.shape["tp"]
    heights = [getattr(d, "coords", (0, 0, i))[2] for i, d in enumerate(mesh.devices[:, 0])]
    X = heights.count(heights[0])
    if n_fs % X:
        X = 1
    Z = n_fs // X
    cores = [getattr(d, "core_on_chip", 0) for d in mesh.devices[0]]
    C = len(set(cores))
    if n_tp % C:
        C = 1
    Y = n_tp // C

    def on_device(tokens, mix_gain, mlp_gain, wq, wk, wv, wg, wo, wu, wd, sq, sk, sv, sg, so, su, sd, forget):
        cfg = Cfg()
        cfg.Z, cfg.X, cfg.Y, cfg.C = Z, X, Y, C
        width, L = tokens.shape
        cfg.width, cfg.L, cfg.D = width, L, width * n_tp
        D = cfg.D
        heads = forget.shape[0]
        G = cfg.G = next(q for q in (4, 2, 1) if Z % q == 0 and heads % q == 0)
        ret = cfg.ret = wq.shape[1]
        cfg.head = ret // heads
        hw = cfg.hw = ret // G
        chunk = cfg.chunk = wu.shape[1] // G
        rows = cfg.rows = wq.shape[0]
        n_dev = n_fs * n_tp
        Q = cfg.Q = 4 if rows % 64 == 0 else 1
        U = cfg.U = 2
        scales = [scale_rows(s) for s in (sq, sk, sv, sg, so, sd, su)]
        n_rows = -(-sum(s.shape[0] for s in scales) // 8) * 8
        gains = [v.reshape(-1, LANES) for v in (mix_gain, mlp_gain)]
        cos_t, sin_t = tables(L, cfg.head)
        vm = pl.BlockSpec(memory_space=pltpu.VMEM)
        hbm = pl.BlockSpec(memory_space=pl.ANY)
        dma = pltpu.SemaphoreType.DMA
        strided = rows % LANES == 0
        vmem = lambda *shape, t=BF: pltpu.VMEM(shape, t)
        stack = (lambda *n: vmem(*n, D)) if strided else (lambda *n: vmem(*n[:-1], n_fs, n[-1], rows))
        wt = width // Q
        tb = cfg.tb = 256 if G * L % (256 * C) == 0 else LANES
        scratch = [
            vmem(D, G * L), vmem(ret * n_tp, G * L), vmem(D, ret * n_tp), stack(4 * hw), stack(U, chunk // U),
            vmem(Q, D // Q, chunk), vmem(G, 4 * hw, rows), vmem(G, U, chunk // U, rows), vmem(G, Q, rows // Q, chunk),
            vmem(rows, ret),
            vmem(4, rows, ret, t=F32), vmem(*wo.shape, t=F32), vmem(*wu.shape, t=F32), vmem(*wd.shape, t=F32),
            vmem(Q, D // Q, G * L), vmem(Q, max(C - 1, 1), Y, wt, G * L), vmem(Q, Y, wt, G * L),
            vmem(Q, max(Y - 1, 1), wt, G * L), vmem(Q, wt, G * L), vmem(Q, G, wt, L),
            vmem(G * L // tb, D, tb), vmem(D, L), vmem(chunk, G * L), vmem(width, L),
            vmem(2, D, LANES, t=F32), vmem(D, LANES, t=F32), vmem(G * chunk, LANES, t=F32),
            vmem(width, LANES, t=F32), vmem(4, ret, LANES, t=F32), vmem(hw // cfg.head, L, L, t=F32),
            vmem(n_dev, n_rows, LANES, t=F32), dma((8,)), dma((2 + U + Q,)),
        ]
        line = lambda n, nx: [(n + 1,), (n,), (n, Y), (n, Y), (n, Y, nx, C), (n, Y, nx, C)]
        W = 1 + U + Q
        shapes = [(n_dev,), (n_dev,), (W, Z), (W, Z), (W, Z, X), (W, Z, X)] + line(G, 1) + line(G, 1)
        first = line(Z, X)
        shapes += first[:4] + [(Z, Y, X), (Z, Y, X)] + first[4:]
        shapes += [(Q, C, Y), (Q, C, Y), (Q, Y), (Q, Y), (Q, G), (Q, G)]
        shapes += [(G * L // tb, C), (G * L // tb, C)]
        scratch += [dma(s) for s in shapes] + [vmem(n_rows, LANES, t=F32)]
        return pl.pallas_call(
            functools.partial(kernel, cfg),
            out_shape=jax.ShapeDtypeStruct((width, L), BF),
            in_specs=[hbm] + [vm] * 4 + [pl.BlockSpec(memory_space=pltpu.SMEM)] + [hbm] * 7 + [vm] * 7,
            out_specs=vm,
            scratch_shapes=scratch,
            compiler_params=pltpu.CompilerParams(
                collective_id=0, has_side_effects=True, vmem_limit_bytes=63 * 2**20
            ),
            name="layer",
        )(tokens, *gains, jnp.asarray(cos_t), jnp.asarray(sin_t), forget, wq, wk, wv, wg, wo, wu, wd, *scales)

    cut = P(("tp", "fs"))
    rows, cols = P("fs", "tp"), P("tp", "fs")
    in_specs = (cols, P(), P(), rows, rows, rows, rows, cols, rows, cols) + (cut,) * 7 + (P("tp"),)
    return jax.shard_map(on_device, mesh=mesh, in_specs=in_specs, out_specs=cols, check_vma=False)
```

time: 201 us -> 164 us (0.82); the launches traced: 198 us -> 163 us
  Pallas kernels: 191 us -> 161 us
  local copies, waits for them, and re-layouts: 5.09 us -> 1.78 us
    pallas_call x1, Pallas kernels: 191 us -> 161 us  [on_device(): pl.pallas_call(functools.partial(kernel, cfg), out_shape=jax.ShapeDtypeSt...]
    broadcast_in_dim x3 -> x0, local copies, waits for them, and re-layouts: 2.02 us -> none  [scale_rows(): return jnp.pad(s, (0, LANES - n))[None, :]]
where the time goes in v3:
time: 164 us; the launch traced here: 163 us
  Pallas kernels  161 us (98%)
  local copies, waits for them, and re-layouts  1.78 us (1%)
    pallas_call x1, Pallas kernels, on_device(): pl.pallas_call(functools.partial(kernel, cfg), out_shape=jax.ShapeDtypeSt...  161 us

profile of v3, /device:TPU:16, one launch (start us, length us, event | category | flops | bytes accessed | tf_op | source)
XLA Modules:
  0.0 163.2 jit_solution(6857095433369601396)
XLA Ops:
  0.0 161.4 %layer.1 = bf16[512,384]{1,0:T(8,128)(2,1)} custom-call(bf16[512,384]{1,0:T(8,128)(2,1)} %refs_0_.1, f32[16,128]{1,0:T(8,128)} %bitcast.9, f32[16,128]{1,0:T(8,128)} %bitcast.10, f32[64,384]{1,0:T(8,128)} %constant.4.clone.refs_3_, f32[64,384]{1,0:T(8,128)} %constant.5.clone.refs_4_, f32[4]{0:T(128)} %refs_5_.1, f32[256,256]{1,0:T(8,128)} %refs_6_.1, ...), custom_call_target="tpu_custom_call" | custom-call | tf_op jit(solution)/shard_map/layer/pallas_call | solution.py:692
  161.4 1.8 %copy.22 = bf16[512,384]{1,0:T(8,128)(2,1)} copy(bf16[512,384]{1,0:T(8,128)(2,1)} %layer.1) | data formatting | bytes 786432

commit v4 on v3

--- a/solution.py
+++ b/solution.py
@@ -231,18 +231,29 @@
 
     locals_ = {}
 
-    def z_send(w, when=None, track=True):
+    def z_send(w, when=None, track=True, ends_too=None):
         copies = []
         for i in range(1, Z):
             to = prj.order(i)
             o = lax.rem(to + Z - z, Z) - 1
             copy = remote(mine(w, lax.rem(to, G)), place(w, me), wzs.at[w, o], wzr.at[w, o], to_z(to))
-            copies.append((copy, None))
+            ok = None
+            if ends_too is not None:
+                ok = (to == 0) | (to == Z - 1)
+                ok = ok if ends_too else jnp.logical_not(ok)
+            copies.append((copy, ok))
         emit([], copies, when, track)
+
+    def from_x(w):
+        n = Z * (X - 1)
+        if w >= DOWN:
+            return f_down.at[w - DOWN, pl.ds(0, n * rq)]
+        ref = f_proj if w == 0 else f_up.at[w - 1]
+        return ref.at[:, pl.ds(0, n * rows)] if strided else ref.at[pl.ds(0, n)]
 
     def x_own(w):
         for o in range(1, X):
-            send(mine(w, g), place(w, me), wxs.at[w, 0, o - 1], wxr.at[w, 0, o - 1], to_x(o))
+            remote(mine(w, g), place(w, me), wxs.at[w], wxr.at[w], to_x(o)).start()
         copy = pltpu.make_async_copy(mine(w, g), place(w, me), local_sem.at[w])
         copy.start()
         locals_[w] = copy
@@ -251,15 +262,12 @@
         for k in range(1, Z):
             piece = place(w, lax.rem(z + Z - k, Z) * X + x)
             wait = remote(piece, piece, wzs.at[w, k - 1], wzr.at[w, k - 1], to_x(1) if X > 1 else to_core(1))
-            emit([wait], [(remote(piece, piece, wxs.at[w, k, o - 1], wxr.at[w, k, o - 1], to_x(o)), None)
-                          for o in range(1, X)], when, track)
+            emit([wait], [(remote(piece, piece, wxs.at[w], wxr.at[w], to_x(o)), None) for o in range(1, X)],
+                 when, False)
 
     def finish(w):
         locals_[w].wait()
-        for k in range(Z):
-            for o in range(1, X):
-                owner = lax.rem(z + Z - k, Z) * X + lax.rem(x + X - o, X)
-                arrived(place(w, owner), wxs.at[w, k, o - 1], wxr.at[w, k, o - 1])
+        arrived(from_x(w), wxs.at[w], wxr.at[w])
 
     def wide(col, n):
         return jnp.concatenate([col] * (n // LANES), axis=1) if n > LANES else col[:, :n]
@@ -300,7 +308,7 @@
         tok.start()
 
         def tell(o, carry):
-            remote(scales, scale_g.at[flat], sc_s.at[o], sc_r.at[o], peer(o)).start()
+            remote(scales, scale_g.at[flat], sc_s.at[0], sc_r.at[0], peer(o)).start()
             return carry
 
         lax.fori_loop(1, n_dev, tell, 0)
@@ -359,14 +367,14 @@
         z_send(0, when=jnp.logical_not(ends), track=False)
         tok.on_y(0)
     with jax.named_scope("scales"):
-        def heard(o, carry):
-            slot = scale_g.at[lax.rem(flat + n_dev - o, n_dev)]
-            arrived(slot, sc_s.at[o], sc_r.at[o])
-            return carry
-
-        lax.fori_loop(1, n_dev, heard, 0)
+        others = scale_g.at[pl.ds(0, n_dev - 1)]
+        arrived(others, sc_s.at[0], sc_r.at[0])
         for i in range(4):
             columns(proj_c.at[i], i, ret // n_fs, n_fs, tp * n_fs)
+    with jax.named_scope("columns"):
+        columns(out_c, 4, D // n_dev, n_dev, 0)
+        columns(down_c, 5, width // n_fs, n_fs, tp * n_fs)
+        columns(up_c, 6, G * chunk // n_fs, n_fs, tp * n_fs)
     inner = jnp.logical_not(ends)
     with jax.named_scope("tok_y1"):
         tok.on_y(1)
@@ -473,10 +481,6 @@
     with jax.named_scope("prj_y3"):
         for k in range(3, Z):
             prj.on_y(k)
-    with jax.named_scope("columns"):
-        columns(out_c, 4, D // n_dev, n_dev, 0)
-        columns(down_c, 5, width // n_fs, n_fs, tp * n_fs)
-        columns(up_c, 6, G * chunk // n_fs, n_fs, tp * n_fs)
     with jax.named_scope("relay1"):
         for w in range(1, 1 + U // 2):
             relay(w)
@@ -576,10 +580,6 @@
             if n == 0:
                 for w in range(1 + U // 2, DOWN):
                     relay(w)
-    with jax.named_scope("keep"):
-        mine_at = rows_of(tp, width)
-        v = nn(out_full[mine_at, :], mix_g[:, seq_at(g)]) * wide(out_c[mine_at, :], L)
-        keep[...] = (tok_g[mine_at, seq_at(g)].astype(F32) + v).astype(BF)
     with jax.named_scope("finish1"):
         for w in range(1, 1 + U):
             finish(w)
@@ -588,22 +588,27 @@
             settled(n)
         relay(DOWN)
         lax.fori_loop(0, n_blocks, expand, 0)
-    for n in range(Q + 1):
+    for n in range(Q + 2):
         with jax.named_scope("down%d" % n):
             if n < Q:
-                with jax.named_scope("drel"):
-                    for w in range(n + 1, Q if n == 1 else n + 2):
-                        if w < Q and n < 2:
-                            relay(DOWN + w)
+                if n + 1 < Q:
+                    with jax.named_scope("drel"):
+                        relay(DOWN + n + 1)
                 with jax.named_scope("dfin"):
                     finish(DOWN + n)
                 with jax.named_scope("shrink"):
                     shrink(n)
+            if 1 <= n <= Q:
                 with jax.named_scope("rcore"):
-                    reduce_core(n)
-            if n:
+                    reduce_core(n - 1)
+            if n == 2:
+                with jax.named_scope("keep"):
+                    mine_at = rows_of(tp, width)
+                    v = nn(out_full[mine_at, :], mix_g[:, seq_at(g)]) * wide(out_c[mine_at, :], L)
+                    keep[...] = (tok_g[mine_at, seq_at(g)].astype(F32) + v).astype(BF)
+            if n >= 2:
                 with jax.named_scope("ry"):
-                    reduce_y(n - 1)
+                    reduce_y(n - 2)
     with jax.named_scope("final"):
         for q in range(Q):
             reduce_z(q)
@@ -613,11 +618,10 @@
         else:
             pl.when(when)(copy.wait_send)
 
-    def told(o, carry):
-        remote(scales, scale_g.at[flat], sc_s.at[o], sc_r.at[o], peer(o)).wait_send()
-        return carry
-
-    lax.fori_loop(1, n_dev, told, 0)
+    others = scale_g.at[pl.ds(0, n_dev - 1)]
+    remote(others, others, sc_s.at[0], sc_r.at[0], peer(1)).wait_send()
+    for w in range(DOWN + Q):
+        remote(from_x(w), from_x(w), wxs.at[w], wxr.at[w], to_x(1)).wait_send()
 
 
 def tables(length, head):
@@ -655,7 +659,7 @@
         chunk = cfg.chunk = wu.shape[1] // G
         rows = cfg.rows = wq.shape[0]
         n_dev = n_fs * n_tp
-        Q = cfg.Q = 4 if rows % 64 == 0 else 1
+        Q = cfg.Q = next(q for q in (8, 4, 2, 1) if rows % (q * 16) == 0)
         U = cfg.U = 2
         scales = [scale_rows(s) for s in (sq, sk, sv, sg, so, sd, su)]
         n_rows = -(-sum(s.shape[0] for s in scales) // 8) * 8
@@ -681,13 +685,14 @@
             vmem(width, LANES, t=F32), vmem(4, ret, LANES, t=F32), vmem(hw // cfg.head, L, L, t=F32),
             vmem(n_dev, n_rows, LANES, t=F32), dma((8,)), dma((2 + U + Q,)),
         ]
-        line = lambda n, nx: [(n + 1,), (n,), (n, Y), (n, Y), (n, Y, nx, C), (n, Y, nx, C)]
+        y1, c1, x1 = max(Y - 1, 1), max(C - 1, 1), max(X - 1, 1)
+        line = lambda n, nx: [(n + 1,), (n,), (n, y1), (n, y1), (n, Y, nx, c1), (n, Y, nx, c1)]
         W = 1 + U + Q
-        shapes = [(n_dev,), (n_dev,), (W, Z), (W, Z), (W, Z, X), (W, Z, X)] + line(G, 1) + line(G, 1)
+        shapes = [(1,), (1,), (W, max(Z - 1, 1)), (W, max(Z - 1, 1)), (W,), (W,)] + line(G, 1) + line(G, 1)
         first = line(Z, X)
-        shapes += first[:4] + [(Z, Y, X), (Z, Y, X)] + first[4:]
-        shapes += [(Q, C, Y), (Q, C, Y), (Q, Y), (Q, Y), (Q, G), (Q, G)]
-        shapes += [(G * L // tb, C), (G * L // tb, C)]
+        shapes += first[:4] + [(Z, Y, x1), (Z, Y, x1)] + first[4:]
+        shapes += [(Q, c1, Y), (Q, c1, Y), (Q, y1), (Q, y1), (Q, G), (Q, G)]
+        shapes += [(G * L // tb // C, c1), (G * L // tb // C, c1)]
         scratch += [dma(s) for s in shapes] + [vmem(n_rows, LANES, t=F32)]
         return pl.pallas_call(
             functools.partial(kernel, cfg),

time: 164 us -> 160 us (0.976)
  Pallas kernels: 161 us -> 157 us
    pallas_call x1, Pallas kernels: 161 us -> 157 us  [on_device(): pl.pallas_call(functools.partial(kernel, cfg), out_shape=jax.ShapeDtypeSt...]
where the time goes in v4:
time: 160 us; the launch traced here: 159 us
  Pallas kernels  157 us (98%)
  local copies, waits for them, and re-layouts  1.78 us (1%)
    pallas_call x1, Pallas kernels, on_device(): pl.pallas_call(functools.partial(kernel, cfg), out_shape=jax.ShapeDtypeSt...  157 us

profile of v4, /device:TPU:16, one launch (start us, length us, event | category | flops | bytes accessed | tf_op | source)
XLA Modules:
  0.0 158.7 jit_solution(4160963528211609366)
XLA Ops:
  0.0 156.9 %layer.1 = bf16[512,384]{1,0:T(8,128)(2,1)} custom-call(bf16[512,384]{1,0:T(8,128)(2,1)} %refs_0_.1, f32[16,128]{1,0:T(8,128)} %bitcast.9, f32[16,128]{1,0:T(8,128)} %bitcast.10, f32[64,384]{1,0:T(8,128)} %constant.4.clone.refs_3_, f32[64,384]{1,0:T(8,128)} %constant.5.clone.refs_4_, f32[4]{0:T(128)} %refs_5_.1, f32[256,256]{1,0:T(8,128)} %refs_6_.1, ...), custom_call_target="tpu_custom_call" | custom-call | tf_op jit(solution)/shard_map/layer/pallas_call | solution.py:697
  157.0 1.8 %copy.22 = bf16[512,384]{1,0:T(8,128)(2,1)} copy(bf16[512,384]{1,0:T(8,128)(2,1)} %layer.1) | data formatting | bytes 786432

commit v5 on v4

--- a/solution.py
+++ b/solution.py
@@ -110,6 +110,8 @@
             src_ref=src, dst_ref=dst, send_sem=ss, recv_sem=rs, device_id=where, device_id_type=MESH
         )
 
+    pooled = []
+
     def emit(waits, copies, when=None, track=True):
         def go():
             for copy in waits:
@@ -125,7 +127,10 @@
         else:
             pl.when(when)(go)
         if track:
-            pending.extend(copies)
+            pending.extend(c for c in copies if not any(c[0] is q for q in pooled))
+
+    def begin(*a):
+        remote(*a).start()
 
     def send(*a):
         emit([], [(remote(*a), None)])
@@ -134,7 +139,8 @@
         remote(ref, ref, ss, rs, to_core(1) if C > 1 else to_z(z)).wait_recv()
 
     class Spread:
-        def __init__(self, n, at, first, ref, zs, zr, ys, yr, cs, cr, xs=None, xr=None):
+        def __init__(self, n, at, first, ref, zs, zr, ys, yr, cs, cr, xs=None, xr=None, pool=None):
+            self.pool = pool
             self.n, self.at, self.first, self.ref = n, at, first, ref
             self.zs, self.zr, self.ys, self.yr, self.cs, self.cr, self.xs, self.xr = zs, zr, ys, yr, cs, cr, xs, xr
             self.nx = X if xs is not None else 1
@@ -159,6 +165,10 @@
 
         def fan_c(self, i, j, k):
             piece = self.block(i, j, k, 0)
+            if self.pool is not None:
+                copies = [remote(piece, piece, self.cs.at[0], self.cr.at[0], to_core(o)) for o in range(1, C)]
+                pooled.extend(copies)
+                return [(copy, None) for copy in copies]
             return [(remote(piece, piece, self.cs.at[i, j, k, o - 1], self.cr.at[i, j, k, o - 1], to_core(o)), None)
                     for o in range(1, C)]
 
@@ -198,6 +208,11 @@
                     arrived(self.block(i, j, k, 0), self.xs.at[i, j, k - 1], self.xr.at[i, j, k - 1])
                     emit([], self.fan_c(i, j, k))
 
+        def all_c(self):
+            if C > 1:
+                arrived(self.pool, self.cs.at[0], self.cr.at[0])
+                pending.append((remote(self.pool, self.pool, self.cs.at[0], self.cr.at[0], to_core(1)), None))
+
         def on_c(self, i):
             for j in range(Y):
                 for k in range(self.nx):
@@ -206,9 +221,9 @@
 
     tok = Spread(G, g, base, lambda zi, xi, t: tok_g.at[rows_of(t, width), seq_at(zi)], t_zs, t_zr, t_ys, t_yr, t_cs, t_cr)
     mix = Spread(G, g, base, lambda zi, xi, t: mix_g.at[pl.ds(pl.multiple_of(t * ret + zi * hw, hw), hw)],
-                 m_zs, m_zr, m_ys, m_yr, m_cs, m_cr)
+                 m_zs, m_zr, m_ys, m_yr, m_cs, m_cr, pool=mix_g.at[pl.ds(0, ret * Y * (C - 1))])
     prj = Spread(Z, z, 0, lambda zi, xi, t: out_full.at[rows_of(zi * X + xi, rows), rows_of(t, ret)],
-                 p_zs, p_zr, p_ys, p_yr, p_cs, p_cr, p_xs, p_xr)
+                 p_zs, p_zr, p_ys, p_yr, p_cs, p_cr, p_xs, p_xr, pool=out_full.at[pl.ds(0, D // C * (C - 1))])
 
     def place(w, owner):
         if w >= DOWN:
@@ -236,16 +251,15 @@
         for i in range(1, Z):
             to = prj.order(i)
             o = lax.rem(to + Z - z, Z) - 1
-            copy = remote(mine(w, lax.rem(to, G)), place(w, me), wzs.at[w, o], wzr.at[w, o], to_z(to))
+            copy = remote(mine(w, lax.rem(to, G)), place(w, me), wzs.at[w], wzr.at[w, o], to_z(to))
             ok = None
             if ends_too is not None:
                 ok = (to == 0) | (to == Z - 1)
                 ok = ok if ends_too else jnp.logical_not(ok)
             copies.append((copy, ok))
-        emit([], copies, when, track)
-
-    def from_x(w):
-        n = Z * (X - 1)
+        emit([], copies, when, False)
+
+    def from_x(w, n=Z * (X - 1)):
         if w >= DOWN:
             return f_down.at[w - DOWN, pl.ds(0, n * rq)]
         ref = f_proj if w == 0 else f_up.at[w - 1]
@@ -261,7 +275,7 @@
     def relay(w, when=None, track=True):
         for k in range(1, Z):
             piece = place(w, lax.rem(z + Z - k, Z) * X + x)
-            wait = remote(piece, piece, wzs.at[w, k - 1], wzr.at[w, k - 1], to_x(1) if X > 1 else to_core(1))
+            wait = remote(piece, piece, wzs.at[w], wzr.at[w, k - 1], to_x(1) if X > 1 else to_core(1))
             emit([wait], [(remote(piece, piece, wxs.at[w], wxr.at[w], to_x(o)), None) for o in range(1, X)],
                  when, False)
 
@@ -494,11 +508,9 @@
         for k in range(Z):
             prj.on_x(k)
     with jax.named_scope("prj_c"):
-        for k in range(Z):
-            prj.on_c(k)
+        prj.all_c()
     with jax.named_scope("mix_c"):
-        for i in range(G):
-            mix.on_c(i)
+        mix.all_c()
 
     tb = cfg.tb
     n_blocks = G * L // tb
@@ -517,9 +529,9 @@
         for o in range(1, C):
             arrived(after.at[n * C + lax.rem(core + C - o, C)], ncs.at[n, o - 1], ncr.at[n, o - 1])
 
-    def expand(b, carry):
+    def expand(i, b, carry):
         at = rows_of(b, tb)
-        for i in range(U):
+        if i < U:
             sc = wide(up_c[pl.ds(pl.multiple_of(g * chunk + i * uh, uh), uh), :], tb)
             u = jnp.maximum(mul(f_up.at[i], after[b]) * sc, 0.0)
             hidden[i * uh : (i + 1) * uh, at] = (u * u).astype(BF)
@@ -537,13 +549,14 @@
         lax.fori_loop(0, G * L // tb, one, 0)
         for o in range(1, C):
             for j in range(Y):
-                send(parts.at[q, rows_of(j * C + lax.rem(core + o, C), wt)], core_in.at[q, o - 1, j],
-                     rcs.at[q, o - 1, j], rcr.at[q, o - 1, j], to_core(o))
+                begin(parts.at[q, rows_of(j * C + lax.rem(core + o, C), wt)], core_in.at[q, o - 1, j],
+                     rcs.at[q, o - 1], rcr.at[q, o - 1], to_core(o))
 
     def reduce_core(q):
         for o in range(1, C):
-            for j in range(Y):
-                arrived(core_in.at[q, o - 1, j], rcs.at[q, o - 1, j], rcr.at[q, o - 1, j])
+            arrived(core_in.at[q, o - 1], rcs.at[q, o - 1], rcr.at[q, o - 1])
+            pending.append((remote(core_in.at[q, o - 1], core_in.at[q, o - 1], rcs.at[q, o - 1], rcr.at[q, o - 1],
+                                   to_core(o)), None))
         for n in range(Y - 1, -1, -1):
             j = lax.rem(y + n, Y)
             value = parts[q, rows_of(j * C + core, wt), :].astype(F32)
@@ -561,14 +574,16 @@
         z_out[q] = value.astype(BF)
         for i in range(G - 1, 0, -1):
             s = tok.order(i)
-            send(z_out.at[q, :, seq_at(s)], z_in.at[q, g], rzs.at[q, i], rzr.at[q, g], to_z(base + s))
+            slot = z_in.at[q, lax.rem(g + G - s, G) - 1]
+            begin(z_out.at[q, :, seq_at(s)], slot, rzs.at[q], rzr.at[q], to_z(base + s))
 
     def reduce_z(q):
         total = z_out[q, :, seq_at(g)].astype(F32)
-        for i in range(1, G):
-            o = tok.order(i)
-            arrived(z_in.at[q, o], rzs.at[q, i], rzr.at[q, o])
-            total += z_in[q, o].astype(F32)
+        if G > 1:
+            arrived(z_in.at[q], rzs.at[q], rzr.at[q])
+            pending.append((remote(z_in.at[q], z_in.at[q], rzs.at[q], rzr.at[q], to_z(base)), None))
+        for i in range(G - 1):
+            total += z_in[q, i].astype(F32)
         for h in range(ppt):
             here = slice(h * rows + q * rq, h * rows + (q + 1) * rq)
             t = total[h * rq : (h + 1) * rq] * wide(down_c[here, :], L)
@@ -581,27 +596,30 @@
                 for w in range(1 + U // 2, DOWN):
                     relay(w)
     with jax.named_scope("finish1"):
-        for w in range(1, 1 + U):
-            finish(w)
+        finish(1)
     with jax.named_scope("expand"):
         for n in range(n_blocks // C):
             settled(n)
-        relay(DOWN)
-        lax.fori_loop(0, n_blocks, expand, 0)
+        for i in range(U):
+            if i:
+                with jax.named_scope("finish2"):
+                    finish(1 + i)
+                relay(DOWN)
+            lax.fori_loop(0, n_blocks, functools.partial(expand, i), 0)
+        relay(DOWN + 1)
     for n in range(Q + 2):
         with jax.named_scope("down%d" % n):
             if n < Q:
-                if n + 1 < Q:
-                    with jax.named_scope("drel"):
-                        relay(DOWN + n + 1)
                 with jax.named_scope("dfin"):
                     finish(DOWN + n)
                 with jax.named_scope("shrink"):
                     shrink(n)
-            if 1 <= n <= Q:
                 with jax.named_scope("rcore"):
-                    reduce_core(n - 1)
-            if n == 2:
+                    reduce_core(n)
+                if n + 2 < Q:
+                    with jax.named_scope("drel"):
+                        relay(DOWN + n + 2)
+            if n == 1:
                 with jax.named_scope("keep"):
                     mine_at = rows_of(tp, width)
                     v = nn(out_full[mine_at, :], mix_g[:, seq_at(g)]) * wide(out_c[mine_at, :], L)
@@ -622,6 +640,7 @@
     remote(others, others, sc_s.at[0], sc_r.at[0], peer(1)).wait_send()
     for w in range(DOWN + Q):
         remote(from_x(w), from_x(w), wxs.at[w], wxr.at[w], to_x(1)).wait_send()
+        remote(from_x(w, Z - 1), from_x(w, Z - 1), wzs.at[w], wxr.at[w], to_x(1)).wait_send()
 
 
 def tables(length, head):
@@ -679,7 +698,7 @@
             vmem(rows, ret),
             vmem(4, rows, ret, t=F32), vmem(*wo.shape, t=F32), vmem(*wu.shape, t=F32), vmem(*wd.shape, t=F32),
             vmem(Q, D // Q, G * L), vmem(Q, max(C - 1, 1), Y, wt, G * L), vmem(Q, Y, wt, G * L),
-            vmem(Q, max(Y - 1, 1), wt, G * L), vmem(Q, wt, G * L), vmem(Q, G, wt, L),
+            vmem(Q, max(Y - 1, 1), wt, G * L), vmem(Q, wt, G * L), vmem(Q, max(G - 1, 1), wt, L),
             vmem(G * L // tb, D, tb), vmem(D, L), vmem(chunk, G * L), vmem(width, L),
             vmem(2, D, LANES, t=F32), vmem(D, LANES, t=F32), vmem(G * chunk, LANES, t=F32),
             vmem(width, LANES, t=F32), vmem(4, ret, LANES, t=F32), vmem(hw // cfg.head, L, L, t=F32),
@@ -688,10 +707,11 @@
         y1, c1, x1 = max(Y - 1, 1), max(C - 1, 1), max(X - 1, 1)
         line = lambda n, nx: [(n + 1,), (n,), (n, y1), (n, y1), (n, Y, nx, c1), (n, Y, nx, c1)]
         W = 1 + U + Q
-        shapes = [(1,), (1,), (W, max(Z - 1, 1)), (W, max(Z - 1, 1)), (W,), (W,)] + line(G, 1) + line(G, 1)
-        first = line(Z, X)
+        pooled = lambda n, nx: line(n, nx)[:4] + [(1,), (1,)]
+        shapes = [(1,), (1,), (W,), (W, max(Z - 1, 1)), (W,), (W,)] + line(G, 1) + pooled(G, 1)
+        first = pooled(Z, X)
         shapes += first[:4] + [(Z, Y, x1), (Z, Y, x1)] + first[4:]
-        shapes += [(Q, c1, Y), (Q, c1, Y), (Q, y1), (Q, y1), (Q, G), (Q, G)]
+        shapes += [(Q, c1), (Q, c1), (Q, y1), (Q, y1), (Q,), (Q,)]
         shapes += [(G * L // tb // C, c1), (G * L // tb // C, c1)]
         scratch += [dma(s) for s in shapes] + [vmem(n_rows, LANES, t=F32)]
         return pl.pallas_call(

time: 160 us -> 157 us (0.981)
  Pallas kernels: 157 us -> 154 us
    pallas_call x1, Pallas kernels: 157 us -> 154 us  [on_device(): pl.pallas_call(functools.partial(kernel, cfg), out_shape=jax.ShapeDtypeSt...]
where the time goes in v5:
time: 157 us; the launch traced here: 156 us
  Pallas kernels  154 us (98%)
  local copies, waits for them, and re-layouts  1.78 us (1%)
    pallas_call x1, Pallas kernels, on_device(): pl.pallas_call(functools.partial(kernel, cfg), out_shape=jax.ShapeDtypeSt...  154 us

profile of v5, /device:TPU:16, one launch (start us, length us, event | category | flops | bytes accessed | tf_op | source)
XLA Modules:
  0.0 155.6 jit_solution(476950961132686843)
XLA Ops:
  0.0 153.8 %layer.1 = bf16[512,384]{1,0:T(8,128)(2,1)} custom-call(bf16[512,384]{1,0:T(8,128)(2,1)} %refs_0_.1, f32[16,128]{1,0:T(8,128)} %bitcast.9, f32[16,128]{1,0:T(8,128)} %bitcast.10, f32[64,384]{1,0:T(8,128)} %constant.4.clone.refs_3_, f32[64,384]{1,0:T(8,128)} %constant.5.clone.refs_4_, f32[4]{0:T(128)} %refs_5_.1, f32[256,256]{1,0:T(8,128)} %refs_6_.1, ...), custom_call_target="tpu_custom_call" | custom-call | tf_op jit(solution)/shard_map/layer/pallas_call | solution.py:717
  153.8 1.8 %copy.22 = bf16[512,384]{1,0:T(8,128)(2,1)} copy(bf16[512,384]{1,0:T(8,128)(2,1)} %layer.1) | data formatting | bytes 786432
